TPU v7x, 32 devices: a whole 2x2x4 slice. The times are simulated.
32 devices in a mesh: sp: 8 (over z, y), tp: 4 (over x, core).
Axes of the slice: x: 2, y: 2, z: 4, core: 2. Of those that a mesh axis runs over, the one named last changes fastest.
Arguments:
- conv_input: bfloat16 [2048, 2048], P('sp', 'tp'), may hold values from -6 to 6
- gate_branch: bfloat16 [2048, 2048], P('sp', 'tp'), may hold values from -6 to 6
- conv_taps: float32 [4, 2048], P(None, 'tp'), may hold values from -3 to 3
- narrow_maps: bfloat16 [2, 8, 128, 128], P(None, 'tp'), may hold values from -0.5 to 0.5
- wide_maps: bfloat16 [2, 4, 256, 256], P(None, 'tp'), may hold values from -0.375 to 0.375
- decay_param: float32 [2048], P('tp'), may hold values from 4.5 to 20
- decay_shift: float32 [2048, 2048], P('sp', 'tp'), may hold values from -0.75 to 0
- mixer_out: bfloat16 [2048, 2048], P('tp'), may hold values from -0.125 to 0.125
- stream: bfloat16 [2048, 2048], P(('sp', 'tp')), may hold values from -6 to 6
- norm_gain: float32 [2048], replicated, may hold values from 0.1 to 1.9
- routes: int32 [2048, 4], P('sp'), may hold values from 0 to 7, all different within a row; in each aligned block of 64 rows (0 to 63, 64 to 127, ...) at most 64 rows name the same one
- route_weights: float32 [2048, 4], P('sp'), may hold values from 0.05 to 0.5
- expert_gate: bfloat16 [8, 2048, 2048], P('sp', None, 'tp'), may hold values from -1 to 1
- expert_up: bfloat16 [8, 2048, 2048], P('sp', None, 'tp'), may hold values from -1 to 1
- expert_down: bfloat16 [8, 2048, 2048], P('sp', 'tp'), may hold values from -0.015625 to 0.015625
Outputs:
- layer_out: bfloat16 [2048, 2048], P(('sp', 'tp'))
Inputs may be any that keep to these rules, and one draw needn't show every extreme that they name: `routes`: each row names 4 different experts. In each aligned block of 64 rows no expert is named more than 64 times, and in every draw some expert is named exactly 64 times in some block.
All inputs are finite; a program needn't handle non-finite values.
Results may differ from a plain program's by a relative error of at most 0.015.
Values may be sent and summed in bfloat16 or wider, within the bound.
A program may use at most 128 MiB of HBM per device.

v0:
```python
import functools

import jax
import jax.numpy as jnp
from jax import lax
from jax.experimental import pallas as pl
from jax.experimental.pallas import tpu as pltpu
from jax.sharding import PartitionSpec as P

NORM_EPSILON = 1e-06
CLAMP_LIMIT = 7.0
GATE_SLOPE = 1.702
DECAY_SCALE = 8.0


def shifted(block, axis, distance):
    devices = range(lax.axis_size(axis))
    route = [(i - distance, i) for i in devices if i - distance in devices]
    return lax.ppermute(block, axis, route)


def clamp_units(gate_pre, up_pre):
    clamped = jnp.minimum(gate_pre, CLAMP_LIMIT)
    upper = jnp.clip(up_pre, -CLAMP_LIMIT, CLAMP_LIMIT)
    return (upper + 1.0) * clamped * jax.nn.sigmoid(GATE_SLOPE * clamped)


def slot_ranks(flat_routes, expert_total):
    onehot = (
        flat_routes[:, :, None] == jnp.arange(expert_total, dtype=jnp.int32)[None, None, :]
    ).astype(jnp.int32)
    return jnp.sum(jnp.cumsum(onehot, axis=1) * onehot, axis=2) - 1


def take_rows(source_rows, slot_source):
    filled = slot_source >= 0
    picked = source_rows[jnp.maximum(slot_source, 0)]
    return jnp.where(filled[:, None], picked, jnp.zeros_like(picked))


def expert_work(arrived, expert_gate, expert_up, expert_down):
    local_experts = expert_gate.shape[0]
    buffer_shape = arrived.shape
    grouped = arrived.reshape(
        buffer_shape[0] // local_experts,
        local_experts,
        buffer_shape[1] * buffer_shape[2],
        buffer_shape[3],
    )
    gate_pre = jnp.einsum(
        "sxcd,xdf->sxcf", grouped, expert_gate, preferred_element_type=jnp.float32
    )
    up_pre = jnp.einsum("sxcd,xdf->sxcf", grouped, expert_up, preferred_element_type=jnp.float32)
    activation = clamp_units(gate_pre, up_pre).astype(jnp.bfloat16)
    partial_value = jnp.einsum(
        "sxcf,xfd->sxcd", activation, expert_down, preferred_element_type=jnp.float32
    )
    return partial_value.reshape(buffer_shape)


LANES = 128
SUBLANES = 8
DX, DY, DC = 1, 2, 4
SERIES_LIMIT = 0.05
GELU_SCALE = 0.7978845608028654
GELU_CUBIC = 0.044715


def mix_kernel(
    head_ref, conv_ref, taps_ref, narrow_ref, wide_ref, soft_ref, shift_ref,
    factor_ref, state_ref, padded, log_keep, drive_keep,
):
    rows, channels = conv_ref.shape
    taps = taps_ref.shape[0]
    padded[0:SUBLANES, :] = head_ref[...]
    padded[SUBLANES:, :] = conv_ref[...].astype(jnp.float32)
    total = jnp.zeros((rows, channels), jnp.float32)
    for k in range(taps):
        total = total + padded[pl.ds(SUBLANES - taps + 1 + k, rows), :] * taps_ref[k : k + 1, :]
    convolved = total.astype(jnp.bfloat16)
    narrow_size, wide_size = narrow_ref.shape[2], wide_ref.shape[2]
    spans = []
    for j in range(wide_ref.shape[1]):
        base = j * (2 * narrow_size + wide_size)
        spans.append((base, narrow_size, narrow_ref, 2 * j))
        spans.append((base + narrow_size, narrow_size, narrow_ref, 2 * j + 1))
        spans.append((base + 2 * narrow_size, wide_size, wide_ref, j))
    for start, size, maps, head in spans:
        piece = convolved[:, start : start + size]
        decay_pre = jnp.dot(piece, maps[0, head], preferred_element_type=jnp.float32)
        input_pre = jnp.dot(piece, maps[1, head], preferred_element_type=jnp.float32)
        cols = slice(start, start + size)
        log_decay = (
            -DECAY_SCALE * jax.nn.sigmoid(decay_pre) * soft_ref[:, cols] + shift_ref[:, cols]
        )
        decay = jnp.exp(log_decay)
        y = 2.0 * log_decay
        series = -y * (1.0 + y * (0.5 + y * (1.0 / 6.0 + y * (1.0 / 24.0 + y * (1.0 / 120.0)))))
        lost = jnp.where(y > -SERIES_LIMIT, series, 1.0 - decay * decay)
        log_keep[:, cols] = decay
        drive_keep[:, cols] = (
            jnp.sqrt(lost) * jax.nn.sigmoid(input_pre) * piece.astype(jnp.float32)
        )
    row_id = lax.broadcasted_iota(jnp.int32, (SUBLANES, channels), 0)

    def tile(i, carry):
        product, state = carry
        at = pl.ds(pl.multiple_of(i * SUBLANES, SUBLANES), SUBLANES)
        a, b = log_keep[at, :], drive_keep[at, :]
        step = 1
        while step < SUBLANES:
            inside = row_id >= step
            a_before = jnp.where(inside, pltpu.roll(a, step, 0), 1.0)
            b_before = jnp.where(inside, pltpu.roll(b, step, 0), 0.0)
            b = a * b_before + b
            a = a * a_before
            step *= 2
        b = b + a * state
        a = a * product
        factor_ref[at, :] = a
        state_ref[at, :] = b
        last = slice(SUBLANES - 1, SUBLANES)
        return (a[last, :], b[last, :])

    lax.fori_loop(
        0,
        rows // SUBLANES,
        tile,
        (jnp.ones((1, channels), jnp.float32), jnp.zeros((1, channels), jnp.float32)),
    )


def mix_local(head, conv_input, conv_taps, narrow_maps, wide_maps, soft, decay_shift):
    shape = conv_input.shape
    flat = jax.ShapeDtypeStruct(shape, jnp.float32)
    return pl.pallas_call(
        mix_kernel,
        out_shape=(flat, flat),
        in_specs=[pl.BlockSpec(memory_space=pltpu.VMEM)] * 7,
        out_specs=(pl.BlockSpec(memory_space=pltpu.VMEM),) * 2,
        scratch_shapes=[
            pltpu.VMEM((shape[0] + SUBLANES, shape[1]), jnp.float32),
            pltpu.VMEM(shape, jnp.float32),
            pltpu.VMEM(shape, jnp.float32),
        ],
        compiler_params=pltpu.CompilerParams(vmem_limit_bytes=32 * 1024 * 1024),
    )(head, conv_input, conv_taps, narrow_maps, wide_maps, soft, decay_shift)


def front_kernel(
    count, conv_ref, gate_ref, taps_ref, narrow_ref, wide_ref, soft_ref, shift_ref, mixer_hbm,
    stream_ref, gain_ref, spread_ref, hid_ref, ext_ref,
    head, factor, state, padded, log_keep, drive_keep, halo, ends, gated, mixer, mix, arrived,
    load_sem, halo_send, halo_recv, end_send, end_recv, mix_send, mix_recv,
):
    rows = conv_ref.shape[0]
    kept, width = stream_ref.shape
    sp, tp = (lax.axis_index("sp"), lax.axis_index("tp"))
    x, c = (tp // 2, tp % 2)
    mesh_id = pl.DeviceIdType.MESH

    def later(k):
        return {"sp": (sp + k) % count, "tp": tp}

    over_x = {"sp": sp, "tp": (1 - x) * 2 + c}
    over_both = {"sp": sp, "tp": (1 - x) * 2 + 1 - c}
    over_c = {"sp": sp, "tp": x * 2 + 1 - c}
    load = pltpu.make_async_copy(mixer_hbm, mixer, load_sem)
    load.start()
    barrier = pltpu.get_barrier_semaphore()
    peers = [over_x, over_both, over_c] + [later(k) for k in range(1, count)]
    for peer in peers:
        pl.semaphore_signal(barrier, inc=1, device_id=peer, device_id_type=mesh_id)
    pl.semaphore_wait(barrier, len(peers))
    halo_rows = halo.shape[0]
    halo_copy = pltpu.make_async_remote_copy(
        src_ref=conv_ref.at[pl.ds(rows - halo_rows, halo_rows)], dst_ref=halo,
        send_sem=halo_send, recv_sem=halo_recv, device_id=later(1), device_id_type=mesh_id,
    )
    halo_copy.start()
    halo_copy.wait()
    before = halo[...].astype(jnp.float32)[halo_rows - SUBLANES :]
    head[...] = jnp.where(sp > 0, before, jnp.zeros_like(before))
    mix_kernel(
        head, conv_ref, taps_ref, narrow_ref, wide_ref, soft_ref, shift_ref,
        factor, state, padded, log_keep, drive_keep,
    )
    ends[0, 0:SUBLANES, :] = factor[rows - SUBLANES :, :]
    ends[0, SUBLANES:, :] = state[rows - SUBLANES :, :]
    end_copies = [
        pltpu.make_async_remote_copy(
            src_ref=ends.at[0], dst_ref=ends.at[k], send_sem=end_send.at[k],
            recv_sem=end_recv.at[k], device_id=later(k), device_id_type=mesh_id,
        )
        for k in range(1, count)
    ]
    for one in end_copies:
        one.start()
    g = gate_ref[...].astype(jnp.float32)
    log_keep[...] = 0.5 * g * (1.0 + jnp.tanh(GELU_SCALE * (g + GELU_CUBIC * g * g * g)))
    load.wait()
    for one in end_copies:
        one.wait()
    last_factor, last_state = (SUBLANES - 1, 2 * SUBLANES - 1)
    carry = jnp.zeros((1, conv_ref.shape[1]), jnp.float32)
    for k in range(count - 1, 0, -1):
        longer = (
            ends[k, last_factor : last_factor + 1, :] * carry
            + ends[k, last_state : last_state + 1, :]
        )
        carry = jnp.where(sp >= k, longer, carry)
    recurrent = state[...] + factor[...] * carry
    gated[...] = (recurrent * log_keep[...]).astype(jnp.bfloat16)

    def project(chip, slot):
        some = gated[pl.ds(pl.multiple_of(chip * 2 * kept, 2 * kept), 2 * kept), :]
        value = jnp.dot(some, mixer[...], preferred_element_type=jnp.float32)
        mix[slot : slot + 2] = value.astype(jnp.bfloat16).reshape(2, kept, width)

    def give(n, source, peer):
        return pltpu.make_async_remote_copy(
            src_ref=mix.at[source], dst_ref=arrived.at[n], send_sem=mix_send.at[n],
            recv_sem=mix_recv.at[n], device_id=peer, device_id_type=mesh_id,
        )

    given = [give(0, c, over_x), give(1, 1 - c, over_both), give(2, 3 - c, over_c)]
    project(1 - x, 0)
    given[0].start()
    given[1].start()
    project(x, 2)
    given[2].start()
    total = mix[2 + c].astype(jnp.float32)
    for n in (2, 0, 1):
        given[n].wait()
        total = total + arrived[n].astype(jnp.float32)
    hidden = (stream_ref[...].astype(jnp.float32) + total).astype(jnp.bfloat16)
    hid_ref[...] = hidden
    wide = hidden.astype(jnp.float32)
    mean = jnp.mean(wide * wide, axis=-1, keepdims=True)
    normed = wide * lax.rsqrt(mean + NORM_EPSILON) * gain_ref[...]
    ext_ref[:, :width] = normed.astype(jnp.bfloat16)
    ext_ref[:, width:] = spread_ref[...]


def front(
    conv_input, gate_branch, conv_taps, narrow_maps, wide_maps, soft, decay_shift, mixer_out,
    stream, norm_gain, spread,
):
    count = lax.axis_size("sp")
    rows, channels = conv_input.shape
    kept, width = stream.shape
    single, kind = (jnp.float32, jnp.bfloat16)
    vmem = pl.BlockSpec(memory_space=pltpu.VMEM)
    dma = pltpu.SemaphoreType.DMA
    return pl.pallas_call(
        functools.partial(front_kernel, count),
        out_shape=(
            jax.ShapeDtypeStruct((kept, width), kind),
            jax.ShapeDtypeStruct((kept, width + LANES), kind),
        ),
        in_specs=[vmem] * 7 + [pl.BlockSpec(memory_space=pl.ANY)] + [vmem] * 3,
        out_specs=(vmem, vmem),
        scratch_shapes=[
            pltpu.VMEM((SUBLANES, channels), single),
            pltpu.VMEM((rows, channels), single),
            pltpu.VMEM((rows, channels), single),
            pltpu.VMEM((rows + SUBLANES, channels), single),
            pltpu.VMEM((rows, channels), single),
            pltpu.VMEM((rows, channels), single),
            pltpu.VMEM((2 * SUBLANES, channels), kind),
            pltpu.VMEM((count, 2 * SUBLANES, channels), single),
            pltpu.VMEM((rows, channels), kind),
            pltpu.VMEM(mixer_out.shape, kind),
            pltpu.VMEM((4, kept, width), kind),
            pltpu.VMEM((3, kept, width), kind),
            dma,
            dma,
            dma,
            dma((count,)),
            dma((count,)),
            dma((3,)),
            dma((3,)),
        ],
        compiler_params=pltpu.CompilerParams(
            collective_id=2, has_side_effects=True, vmem_limit_bytes=40 * 1024 * 1024
        ),
    )(
        conv_input, gate_branch, conv_taps, narrow_maps, wide_maps, soft, decay_shift, mixer_out,
        stream, norm_gain, spread,
    )


def moe_kernel(
    depth, ext_ref, hid_ref, gate_hbm, up_hbm, down_hbm, out_ref,
    xs, part, from_core, from_y, from_x, last_x, last_y, from_z, gate_w, up_w, down_w,
    load_sem, z_send, z_recv, g_send, g_recv, r_send, r_recv, e_send, e_recv,
):
    rows, width = hid_ref.shape
    half = width // 2
    wide = xs.shape[-1]
    sp, tp = (lax.axis_index("sp"), lax.axis_index("tp"))
    z, y = (sp // 2, sp % 2)
    x, c = (tp // 2, tp % 2)
    peer_c = {"sp": sp, "tp": x * 2 + 1 - c}
    peer_x = {"sp": sp, "tp": (1 - x) * 2 + c}
    peer_y = {"sp": z * 2 + 1 - y, "tp": tp}

    def peer_z(k):
        return {"sp": ((z + k) % depth) * 2 + y, "tp": tp}

    def copy(src, dst, send, recv, peer):
        return pltpu.make_async_remote_copy(
            src_ref=src, dst_ref=dst, send_sem=send, recv_sem=recv,
            device_id=peer, device_id_type=pl.DeviceIdType.MESH,
        )

    cols_a, cols_b = (pl.ds(0, half), pl.ds(half, wide - half))
    sum_a, sum_b = (pl.ds(0, half), pl.ds(half, half))
    every = pl.ds(0, rows)

    def ag(k, n):
        sems = (g_send.at[k, n], g_recv.at[k, n])
        if n == 0:
            return copy(xs.at[k, 0], xs.at[k, DX], *sems, peer_x)
        if n == 1:
            return copy(xs.at[k, 0], xs.at[k, DY], *sems, peer_y)
        if n == 2:
            return copy(
                xs.at[k, DX, every, cols_a], xs.at[k, DX + DY, every, cols_a], *sems, peer_y
            )
        if n == 3:
            return copy(
                xs.at[k, DY, every, cols_b], xs.at[k, DX + DY, every, cols_b], *sems, peer_x
            )
        return copy(xs.at[k, n - 4], xs.at[k, DC + n - 4], *sems, peer_c)

    def zg(k):
        return copy(xs.at[0, 0], xs.at[k, 0], z_send.at[k], z_recv.at[k], peer_z(k))

    def rs(k, n):
        sems = (r_send.at[k, n], r_recv.at[k, n])
        if n == 0:
            return copy(part.at[k, pl.ds(DC, DC)], from_core.at[k], *sems, peer_c)
        if n == 1:
            return copy(part.at[k, DY, every, sum_a], from_y.at[k, 0], *sems, peer_y)
        if n == 2:
            return copy(part.at[k, DX + DY, every, sum_a], from_y.at[k, 1], *sems, peer_y)
        if n == 3:
            return copy(part.at[k, DX, every, sum_b], from_x.at[k, 0], *sems, peer_x)
        if n == 4:
            return copy(part.at[k, DX + DY, every, sum_b], from_x.at[k, 1], *sems, peer_x)
        if n == 5:
            return copy(part.at[k, DX, every, sum_a], last_x.at[k], *sems, peer_x)
        return copy(part.at[k, DY, every, sum_b], last_y.at[k], *sems, peer_y)

    def zr(k):
        return copy(part.at[k, 0], from_z.at[k], e_send.at[k], e_recv.at[k], peer_z(depth - k))

    def added(slot, columns, arrived):
        k, s = slot
        now = part[k, s, :, columns].astype(jnp.float32) + arrived.astype(jnp.float32)
        part[k, s, :, columns] = now.astype(jnp.bfloat16)

    loads = [
        pltpu.make_async_copy(gate_hbm.at[0], gate_w, load_sem.at[0]),
        pltpu.make_async_copy(up_hbm.at[0], up_w, load_sem.at[1]),
        pltpu.make_async_copy(down_hbm.at[0], down_w, load_sem.at[2]),
    ]
    own = pltpu.make_async_copy(ext_ref, xs.at[0, 0], load_sem.at[3])
    own.start()
    barrier = pltpu.get_barrier_semaphore()
    peers = [peer_c, peer_x, peer_y] + [peer_z(k) for k in range(1, depth)]
    for peer in peers:
        pl.semaphore_signal(barrier, inc=1, device_id=peer, device_id_type=pl.DeviceIdType.MESH)
    pl.semaphore_wait(barrier, len(peers))
    own.wait()
    for n in (0, 1, 4):
        ag(0, n).start()
    for k in range(1, depth):
        zg(k).start()
    for load in loads:
        load.start()

    block = 4
    lane = lax.broadcasted_iota(jnp.int32, (block * rows, LANES), 1)
    chosen = (lane == sp) | (lane == sp + LANES // 2)

    def compute(k):
        def chunk(i, none):
            j = 1 - i
            held = xs[k, pl.ds(j * block, block)].reshape(block * rows, wide)
            rows_in = held[:, :width]
            weight = jnp.sum(
                jnp.where(chosen, held[:, width:].astype(jnp.float32), 0.0), axis=1, keepdims=True
            )
            g = jnp.dot(rows_in, gate_w[...], preferred_element_type=jnp.float32)
            u = jnp.dot(rows_in, up_w[...], preferred_element_type=jnp.float32)
            act = (clamp_units(g, u) * weight).astype(jnp.bfloat16)
            down = jnp.dot(act, down_w[...], preferred_element_type=jnp.float32)
            part[k, pl.ds(j * block, block)] = down.astype(jnp.bfloat16).reshape(
                block, rows, width
            )

            @pl.when(i == 0)
            def _():
                rs(k, 0).start()

            return none

        lax.fori_loop(0, 2, chunk, 0)

    def step(k, none):
        live, late = (k < depth, k > 0)

        @pl.when(live)
        def _():
            ag(k, 0).wait_recv()
            ag(k, 1).wait_recv()
            for n in (2, 3, 4 + DX, 4 + DY):
                ag(k, n).start()

        @pl.when(k + 1 < depth)
        def _():
            zg(k + 1).wait_recv()
            for n in (0, 1, 4):
                ag(k + 1, n).start()

        @pl.when(live)
        def _():
            ag(k, 2).wait_recv()
            ag(k, 3).wait_recv()
            ag(k, 4 + DX + DY).start()

        @pl.when(late)
        def _():
            p = k - 1
            for n in (1, 2, 3, 4):
                rs(p, n).wait_recv()
            added((p, DX), slice(0, half), from_y[p, 1])
            added((p, DY), slice(half, width), from_x[p, 1])
            rs(p, 5).start()
            rs(p, 6).start()
            added((p, 0), slice(0, half), from_y[p, 0])
            added((p, 0), slice(half, width), from_x[p, 0])

        @pl.when(k == 0)
        def _():
            for load in loads:
                load.wait()

        @pl.when(live)
        def _():
            for n in (4, 5, 6, 7):
                ag(k, n).wait_recv()
            compute(k)
            rs(k, 0).wait_recv()
            for s in range(DC):
                added((k, s), slice(0, width), from_core[k, s])
            for n in (1, 2, 3, 4):
                rs(k, n).start()

        @pl.when(late)
        def _():
            p = k - 1
            rs(p, 5).wait_recv()
            rs(p, 6).wait_recv()
            added((p, 0), slice(0, half), last_x[p])
            added((p, 0), slice(half, width), last_y[p])

        @pl.when(k > 1)
        def _():
            zr(k - 1).start()

        return none

    lax.fori_loop(0, depth + 1, step, 0)
    total = hid_ref[...].astype(jnp.float32) + part[0, 0].astype(jnp.float32)
    for k in range(1, depth):
        zr(k).wait_recv()
        total = total + from_z[k].astype(jnp.float32)
    out_ref[...] = total.astype(out_ref.dtype)

    def drain(k, none):
        for n in range(8):
            ag(k, n).wait_send()
        for n in range(7):
            rs(k, n).wait_send()
        return none

    lax.fori_loop(0, depth, drain, 0)
    for k in range(1, depth):
        zg(k).wait_send()
        zr(k).wait_send()


def experts(ext, hidden, expert_gate, expert_up, expert_down):
    depth = lax.axis_size("sp") // 2
    rows, width = hidden.shape
    wide = ext.shape[1]
    kind = jnp.bfloat16
    vmem = pl.BlockSpec(memory_space=pltpu.VMEM)
    hbm = pl.BlockSpec(memory_space=pl.ANY)
    half = width // 2
    dma = pltpu.SemaphoreType.DMA
    return pl.pallas_call(
        functools.partial(moe_kernel, depth),
        out_shape=jax.ShapeDtypeStruct(hidden.shape, kind),
        in_specs=[vmem, vmem, hbm, hbm, hbm],
        out_specs=vmem,
        scratch_shapes=[
            pltpu.VMEM((depth, 8, rows, wide), kind),
            pltpu.VMEM((depth, 8, rows, width), kind),
            pltpu.VMEM((depth, 4, rows, width), kind),
            pltpu.VMEM((depth, 2, rows, half), kind),
            pltpu.VMEM((depth, 2, rows, half), kind),
            pltpu.VMEM((depth, rows, half), kind),
            pltpu.VMEM((depth, rows, half), kind),
            pltpu.VMEM((depth, rows, width), kind),
            pltpu.VMEM(expert_gate.shape[1:], kind),
            pltpu.VMEM(expert_up.shape[1:], kind),
            pltpu.VMEM(expert_down.shape[1:], kind),
            dma((4,)),
            dma((depth,)),
            dma((depth,)),
            dma((depth, 8)),
            dma((depth, 8)),
            dma((depth, 7)),
            dma((depth, 7)),
            dma((depth,)),
            dma((depth,)),
        ],
        compiler_params=pltpu.CompilerParams(
            collective_id=1, has_side_effects=True, vmem_limit_bytes=56 * 1024 * 1024
        ),
    )(ext, hidden, expert_gate, expert_up, expert_down)


def shards(
    conv_input,
    gate_branch,
    conv_taps,
    narrow_maps,
    wide_maps,
    decay_param,
    decay_shift,
    mixer_out,
    stream,
    norm_gain,
    routes,
    route_weights,
    expert_gate,
    expert_up,
    expert_down,
):
    seq_rows, channels = conv_input.shape
    tap_count = conv_taps.shape[0]
    tp_count = lax.axis_size("tp")
    tok_local = seq_rows // tp_count
    top_count = routes.shape[1]
    expert_total = expert_gate.shape[0] * lax.axis_size("sp")
    capacity = max(2, 2 * tok_local * top_count // expert_total)
    own_index = lax.axis_index("tp")
    own_rows = lax.dynamic_slice_in_dim(routes, own_index * tok_local, tok_local, 0)
    own_weights = lax.dynamic_slice_in_dim(route_weights, own_index * tok_local, tok_local, 0)
    soft = jax.nn.softplus(-decay_param)[None, :]
    whole_rows = capacity >= tok_local and expert_gate.shape[0] == 1
    if whole_rows and tp_count == 4 and lax.axis_size("sp") % 2 == 0:
        lane = jnp.arange(LANES, dtype=jnp.int32)
        spread = jnp.sum(
            jnp.where(
                own_rows[:, :, None] == (lane % (LANES // 2))[None, None, :],
                own_weights[:, :, None],
                0.0,
            ),
            axis=1,
        )
        high = lax.reduce_precision(spread, exponent_bits=8, mantissa_bits=7)
        pair = jnp.where(lane[None, :] < LANES // 2, high, spread - high).astype(jnp.bfloat16)
        hidden, ext = front(
            conv_input, gate_branch, conv_taps, narrow_maps, wide_maps, soft, decay_shift,
            mixer_out, stream, norm_gain[None, :], pair,
        )
        return experts(ext, hidden, expert_gate, expert_up, expert_down)
    earlier = shifted(conv_input[seq_rows - tap_count + 1 :], "sp", 1)
    head = jnp.zeros((SUBLANES, channels), jnp.float32)
    head = head.at[SUBLANES - tap_count + 1 :].set(earlier.astype(jnp.float32))
    factors, local_state = mix_local(
        head, conv_input, conv_taps, narrow_maps, wide_maps, soft, decay_shift
    )
    ends = lax.all_gather(jnp.stack([factors[-1], local_state[-1]]), "sp")
    mine = lax.axis_index("sp")
    state = jnp.zeros((channels,), jnp.float32)
    for position in range(lax.axis_size("sp") - 1):
        longer = ends[position, 0] * state + ends[position, 1]
        state = jnp.where(position < mine, longer, state)
    carried = (None, state)
    recurrent = local_state + factors * carried[1]
    gated_rows = (recurrent * jax.nn.gelu(gate_branch.astype(jnp.float32))).astype(jnp.bfloat16)
    mixer_sum = lax.psum_scatter(
        jnp.dot(gated_rows, mixer_out, preferred_element_type=jnp.float32).astype(jnp.bfloat16),
        "tp",
        scatter_dimension=0,
        tiled=True,
    ).astype(jnp.float32)
    hidden_f = stream.astype(jnp.float32) + mixer_sum
    hidden = hidden_f.astype(jnp.bfloat16)
    hidden_f = hidden.astype(jnp.float32)
    normed = (
        hidden_f
        * lax.rsqrt(jnp.mean(hidden_f * hidden_f, axis=-1, keepdims=True) + NORM_EPSILON)
        * norm_gain
    ).astype(jnp.bfloat16)
    model_width = normed.shape[1]
    assignments = tok_local * top_count
    own_routes = own_rows.reshape(assignments)
    own_ranks = slot_ranks(own_routes[None, :], expert_total)[0]
    source = jnp.arange(assignments, dtype=jnp.int32) // top_count
    slot_source = (
        jnp.full((expert_total * capacity,), -1, jnp.int32)
        .at[own_routes * capacity + own_ranks]
        .set(source)
    )
    outgoing = take_rows(normed, slot_source).reshape(expert_total, 1, capacity, model_width)
    partial_value = expert_work(
        lax.all_gather(
            lax.all_to_all(outgoing, "sp", split_axis=0, concat_axis=0, tiled=True),
            "tp",
            axis=1,
            tiled=True,
        ),
        expert_gate,
        expert_up,
        expert_down,
    )
    summed = lax.psum_scatter(
        partial_value.astype(jnp.bfloat16), "tp", scatter_dimension=1, tiled=True
    )
    returned = lax.all_to_all(summed, "sp", split_axis=0, concat_axis=0, tiled=True)
    own_slots = own_routes * capacity + own_ranks
    picked = returned.reshape(expert_total * capacity, model_width)[own_slots]
    combined = jnp.sum(
        picked.reshape(tok_local, top_count, model_width).astype(jnp.float32)
        * own_weights[:, :, None],
        axis=1,
    )
    return (hidden_f + combined).astype(jnp.bfloat16)


def solution(mesh):
    placed = (
        P("sp", "tp"),
        P("sp", "tp"),
        P(None, "tp"),
        P(None, "tp", None, None),
        P(None, "tp", None, None),
        P("tp"),
        P("sp", "tp"),
        P("tp", None),
        P(("sp", "tp"), None),
        P(),
        P("sp", None),
        P("sp", None),
        P("sp", None, "tp"),
        P("sp", None, "tp"),
        P("sp", "tp", None),
    )
    return jax.shard_map(
        shards, mesh=mesh, in_specs=placed, out_specs=P(("sp", "tp"), None), check_vma=False
    )
```

profile of v0, /device:TPU:0, one launch (start us, length us, event | category | flops | bytes accessed | tf_op | source)
XLA Modules:
  0.0 138.9 jit_solution(907161646541683624)
XLA Ops:
  0.0 0.0 copy-start
  0.0 0.7 compare_select_fusion
  0.7 0.0 copy-done
  0.7 0.1 constant_dynamic-slice_fusion.1
  0.8 0.8 constant_dynamic-slice_fusion
  1.5 0.1 select_reduce_fusion
  1.7 0.0 copy-start.1
  1.7 1.6 %copy-done.1 = bf16[512,2048]{1,0:T(8,128)(2,1)S(1)} copy-done((bf16[512,2048]{1,0:T(8,128)(2,1)S(1)}, bf16[512,2048]{1,0:T(8,128)(2,1)}, u32[]{:S(2)}) %copy-start.1) | copy-done | bytes 2097176
  3.3 0.0 copy-start.2
  3.3 1.0 copy-done.2
  4.3 0.0 copy-start.5
  4.3 0.9 copy-done.5
  5.3 0.0 copy-start.6
  5.3 0.9 copy-done.6
  6.2 0.0 copy-start.7
  6.2 0.9 copy-done.7
  7.2 0.0 copy-start.8
  7.2 0.9 copy-done.8
  8.1 0.0 copy-start.9
  8.1 0.9 copy-done.9
  9.0 0.0 copy-start.10
  9.0 0.7 copy-done.10
  9.7 0.0 copy-start.11
  9.7 0.7 copy-done.11
  10.4 26.4 %shard_map.145 = (bf16[64,2048]{1,0:T(8,128)(2,1)S(1)}, bf16[64,2176]{1,0:T(8,128)(2,1)S(1)}) custom-call(bf16[256,512]{1,0:T(8,128)(2,1)S(1)} %copy-done.5, bf16[256,512]{1,0:T(8,128)(2,1)S(1)} %copy-done.6, f32[4,512]{1,0:T(4,128)S(1)} %copy-done.10, bf16[2,2,128,128]{3,2,1,0:T(8,128)(2,1)S(1)} %copy-done.9, bf16[2,1,256,256]{3,2,1,0:T(8,128)(2,1)S(1)} %copy-done.7, ...), custom_call_target="tpu_custom_call" | custom-call | tf_op jit(solution)/shard_map/pallas_call | solution.py:255
  36.9 0.0 copy-start.3
  36.9 0.7 copy-done.3
  37.6 0.0 copy-start.4
  37.6 0.7 copy-done.4
  38.3 98.9 %shard_map.146 = bf16[64,2048]{1,0:T(8,128)(2,1)} custom-call(bf16[64,2176]{1,0:T(8,128)(2,1)} %copy-done.3, bf16[64,2048]{1,0:T(8,128)(2,1)} %copy-done.4, bf16[1,2048,512]{2,1,0:T(8,128)(2,1)} %gate_hbm.1, bf16[1,2048,512]{2,1,0:T(8,128)(2,1)} %up_hbm.1, bf16[1,512,2048]{2,1,0:T(8,128)(2,1)} %down_hbm.1), custom_call_target="tpu_custom_call" | custom-call | tf_op jit(solution)/shard_map/pallas_call | solution.py:505
  137.2 1.7 %copy.19 = bf16[64,2048]{1,0:T(8,128)(2,1)} copy(bf16[64,2048]{1,0:T(8,128)(2,1)} %shard_map.146) | data formatting | bytes 524288
  (3 shorter events, 0.0 us)
Async XLA Ops:
  0.0 0.7 copy-start
  1.7 1.6 %copy-start.1 = (bf16[512,2048]{1,0:T(8,128)(2,1)S(1)}, bf16[512,2048]{1,0:T(8,128)(2,1)}, u32[]{:S(2)}) copy-start(bf16[512,2048]{1,0:T(8,128)(2,1)} %mixer_hbm.1) | copy-start | bytes 6291460
  3.3 1.0 copy-start.2
  4.3 0.9 copy-start.5
  5.3 0.9 copy-start.6
  6.2 0.9 copy-start.7
  7.2 0.9 copy-start.8
  8.1 0.9 copy-start.9
  9.0 0.7 copy-start.10
  9.7 0.7 copy-start.11
  36.9 0.7 copy-start.3
  37.6 0.7 copy-start.4
where the time goes:
time: 140 us; the launch traced here: 139 us
  Pallas kernels  125 us (89%)
  local copies, waits for them, and re-layouts  12.6 us (9%)
    pallas_call x1, Pallas kernels, experts(): pl.pallas_call(functools.partial(moe_kernel, depth), out_shape=jax.ShapeD...  98.9 us
    pallas_call x1, Pallas kernels, front(): pl.pallas_call(functools.partial(front_kernel, count), out_shape=(jax.Sha...  26.4 us
    unnamed x25, local copies, waits for them, and re-layouts  11.8 us

commit v1 on v0

v1 whole, which is shorter than its diff:
```python
import functools
import types

import jax
import jax.numpy as jnp
from jax import lax
from jax.experimental import pallas as pl
from jax.experimental.pallas import tpu as pltpu
from jax.sharding import PartitionSpec as P

NORM_EPSILON = 1e-06
CLAMP_LIMIT = 7.0
GATE_SLOPE = 1.702
DECAY_SCALE = 8.0


def shifted(block, axis, distance):
    devices = range(lax.axis_size(axis))
    route = [(i - distance, i) for i in devices if i - distance in devices]
    return lax.ppermute(block, axis, route)


def clamp_units(gate_pre, up_pre):
    clamped = jnp.minimum(gate_pre, CLAMP_LIMIT)
    upper = jnp.clip(up_pre, -CLAMP_LIMIT, CLAMP_LIMIT)
    return (upper + 1.0) * clamped * jax.nn.sigmoid(GATE_SLOPE * clamped)


def slot_ranks(flat_routes, expert_total):
    onehot = (
        flat_routes[:, :, None] == jnp.arange(expert_total, dtype=jnp.int32)[None, None, :]
    ).astype(jnp.int32)
    return jnp.sum(jnp.cumsum(onehot, axis=1) * onehot, axis=2) - 1


def take_rows(source_rows, slot_source):
    filled = slot_source >= 0
    picked = source_rows[jnp.maximum(slot_source, 0)]
    return jnp.where(filled[:, None], picked, jnp.zeros_like(picked))


def expert_work(arrived, expert_gate, expert_up, expert_down):
    local_experts = expert_gate.shape[0]
    buffer_shape = arrived.shape
    grouped = arrived.reshape(
        buffer_shape[0] // local_experts,
        local_experts,
        buffer_shape[1] * buffer_shape[2],
        buffer_shape[3],
    )
    gate_pre = jnp.einsum(
        "sxcd,xdf->sxcf", grouped, expert_gate, preferred_element_type=jnp.float32
    )
    up_pre = jnp.einsum("sxcd,xdf->sxcf", grouped, expert_up, preferred_element_type=jnp.float32)
    activation = clamp_units(gate_pre, up_pre).astype(jnp.bfloat16)
    partial_value = jnp.einsum(
        "sxcf,xfd->sxcd", activation, expert_down, preferred_element_type=jnp.float32
    )
    return partial_value.reshape(buffer_shape)


LANES = 128
SUBLANES = 8
DX, DY, DC = 1, 2, 4
SERIES_LIMIT = 0.05
GELU_SCALE = 0.7978845608028654
GELU_CUBIC = 0.044715


def mix_kernel(
    head_ref, conv_ref, taps_ref, narrow_ref, wide_ref, soft_ref, shift_ref,
    factor_ref, state_ref, padded, log_keep, drive_keep,
):
    rows, channels = conv_ref.shape
    taps = taps_ref.shape[0]
    padded[0:SUBLANES, :] = head_ref[...]
    padded[SUBLANES:, :] = conv_ref[...].astype(jnp.float32)
    total = jnp.zeros((rows, channels), jnp.float32)
    for k in range(taps):
        total = total + padded[pl.ds(SUBLANES - taps + 1 + k, rows), :] * taps_ref[k : k + 1, :]
    convolved = total.astype(jnp.bfloat16)
    narrow_size, wide_size = narrow_ref.shape[2], wide_ref.shape[2]
    spans = []
    for j in range(wide_ref.shape[1]):
        base = j * (2 * narrow_size + wide_size)
        spans.append((base, narrow_size, narrow_ref, 2 * j))
        spans.append((base + narrow_size, narrow_size, narrow_ref, 2 * j + 1))
        spans.append((base + 2 * narrow_size, wide_size, wide_ref, j))
    for start, size, maps, head in spans:
        piece = convolved[:, start : start + size]
        decay_pre = jnp.dot(piece, maps[0, head], preferred_element_type=jnp.float32)
        input_pre = jnp.dot(piece, maps[1, head], preferred_element_type=jnp.float32)
        cols = slice(start, start + size)
        log_decay = (
            -DECAY_SCALE * jax.nn.sigmoid(decay_pre) * soft_ref[:, cols] + shift_ref[:, cols]
        )
        decay = jnp.exp(log_decay)
        y = 2.0 * log_decay
        series = -y * (1.0 + y * (0.5 + y * (1.0 / 6.0 + y * (1.0 / 24.0 + y * (1.0 / 120.0)))))
        lost = jnp.where(y > -SERIES_LIMIT, series, 1.0 - decay * decay)
        log_keep[:, cols] = decay
        drive_keep[:, cols] = (
            jnp.sqrt(lost) * jax.nn.sigmoid(input_pre) * piece.astype(jnp.float32)
        )
    row_id = lax.broadcasted_iota(jnp.int32, (SUBLANES, channels), 0)

    def tile(i, carry):
        product, state = carry
        at = pl.ds(pl.multiple_of(i * SUBLANES, SUBLANES), SUBLANES)
        a, b = log_keep[at, :], drive_keep[at, :]
        step = 1
        while step < SUBLANES:
            inside = row_id >= step
            a_before = jnp.where(inside, pltpu.roll(a, step, 0), 1.0)
            b_before = jnp.where(inside, pltpu.roll(b, step, 0), 0.0)
            b = a * b_before + b
            a = a * a_before
            step *= 2
        b = b + a * state
        a = a * product
        factor_ref[at, :] = a
        state_ref[at, :] = b
        last = slice(SUBLANES - 1, SUBLANES)
        return (a[last, :], b[last, :])

    lax.fori_loop(
        0,
        rows // SUBLANES,
        tile,
        (jnp.ones((1, channels), jnp.float32), jnp.zeros((1, channels), jnp.float32)),
    )


def mix_local(head, conv_input, conv_taps, narrow_maps, wide_maps, soft, decay_shift):
    shape = conv_input.shape
    flat = jax.ShapeDtypeStruct(shape, jnp.float32)
    return pl.pallas_call(
        mix_kernel,
        out_shape=(flat, flat),
        in_specs=[pl.BlockSpec(memory_space=pltpu.VMEM)] * 7,
        out_specs=(pl.BlockSpec(memory_space=pltpu.VMEM),) * 2,
        scratch_shapes=[
            pltpu.VMEM((shape[0] + SUBLANES, shape[1]), jnp.float32),
            pltpu.VMEM(shape, jnp.float32),
            pltpu.VMEM(shape, jnp.float32),
        ],
        compiler_params=pltpu.CompilerParams(vmem_limit_bytes=32 * 1024 * 1024),
    )(head, conv_input, conv_taps, narrow_maps, wide_maps, soft, decay_shift)


def nearest(z, p, depth):
    short = jnp.minimum(z, depth - 1 - z)
    near = p <= 2 * short
    distance = jnp.where(near, (p + 1) // 2, p - short)
    left = jnp.where(near, p % 2, jnp.where(z > depth - 1 - z, 1, 0))
    return jnp.where(p == 0, 0, jnp.where(left == 1, distance, depth - distance))


def layer_kernel(count, names, *refs):
    v = types.SimpleNamespace(**dict(zip(names, refs)))
    rows, channels = v.conv.shape
    kept, width = v.stream.shape
    depth = count // 2
    half = kept // 2
    single, kind = (jnp.float32, jnp.bfloat16)
    sp, tp = (lax.axis_index("sp"), lax.axis_index("tp"))
    z, y = (sp // 2, sp % 2)
    x, c = (tp // 2, tp % 2)
    mesh_id = pl.DeviceIdType.MESH
    peer_c = {"sp": sp, "tp": x * 2 + 1 - c}
    peer_x = {"sp": sp, "tp": (1 - x) * 2 + c}
    peer_y = {"sp": z * 2 + 1 - y, "tp": tp}

    def plane(k):
        return {"sp": ((z + k) % depth) * 2 + y, "tp": tp}

    def later(k):
        return {"sp": (sp + k) % count, "tp": tp}

    def copy(src, dst, send, recv, peer):
        return pltpu.make_async_remote_copy(
            src_ref=src, dst_ref=dst, send_sem=send, recv_sem=recv,
            device_id=peer, device_id_type=mesh_id,
        )

    barrier = pltpu.get_barrier_semaphore()
    peers = [peer_x, peer_c] + [later(k) for k in range(1, count)]
    for peer in peers:
        pl.semaphore_signal(barrier, inc=1, device_id=peer, device_id_type=mesh_id)
    load_names = (
        "conv", "taps", "narrow", "wide", "decay", "shift", "gate", "routes", "shares", "stream",
        "gain", "mixer", "gate_w", "up_w", "down_w",
    )
    loads = {}
    for n, name in enumerate(load_names):
        source = getattr(v, name + "_hbm")
        source = source.at[0] if name.endswith("_w") else source
        loads[name] = pltpu.make_async_copy(source, getattr(v, name), v.load_sem.at[n])
        loads[name].start()

    loads["conv"].wait()
    pl.semaphore_wait(barrier, len(peers))
    halo_rows = v.halo.shape[0]
    halo_copy = copy(
        v.conv.at[pl.ds(rows - halo_rows, halo_rows)], v.halo, v.halo_send, v.halo_recv, later(1)
    )
    halo_copy.start()

    loads["routes"].wait()
    loads["shares"].wait()
    lines = v.weigh_out.shape[1]
    line = lax.broadcasted_iota(jnp.int32, (lines, rows), 0)
    for e in range(count):
        share = jnp.zeros((1, rows), single)
        for n in range(v.routes.shape[0]):
            share = share + jnp.where(
                v.routes[n : n + 1, :] == e, v.shares[n : n + 1, :], 0.0
            )
        v.weigh_out[e] = jnp.where(line == sp, share, 0.0)
    weigh_copies = [
        copy(
            v.weigh_out.at[(sp + k) % count], v.weigh_in.at[k], v.weigh_send.at[k],
            v.weigh_recv.at[k], later(k),
        )
        for k in range(1, count)
    ]
    for one in weigh_copies:
        one.start()

    loads["decay"].wait()
    t = jnp.exp(-v.decay[...])
    v.soft[...] = t * (1.0 - t * (0.5 - t * (1.0 / 3.0 - t * (0.25 - t * (0.2 - t * (1.0 / 6.0))))))
    loads["gate"].wait()
    g = v.gate[...].astype(single)
    v.gelu[...] = 0.5 * g * (1.0 + jnp.tanh(GELU_SCALE * (g + GELU_CUBIC * g * g * g)))
    for name in ("taps", "narrow", "wide", "shift"):
        loads[name].wait()

    halo_copy.wait()
    before = v.halo[...].astype(single)[halo_rows - SUBLANES :]
    v.head[...] = jnp.where(sp > 0, before, jnp.zeros_like(before))
    mix_kernel(
        v.head, v.conv, v.taps, v.narrow, v.wide, v.soft, v.shift,
        v.factor, v.state, v.padded, v.log_keep, v.drive_keep,
    )
    groups = channels // LANES
    for n in range(groups):
        cols = slice(n * LANES, (n + 1) * LANES)
        v.ends[0, n : n + 1, :] = v.factor[rows - 1 : rows, cols]
        v.ends[0, groups + n : groups + n + 1, :] = v.state[rows - 1 : rows, cols]
    end_copies = [
        copy(v.ends.at[0], v.ends.at[k], v.end_send.at[k], v.end_recv.at[k], later(k))
        for k in range(1, count)
    ]
    for one in end_copies:
        one.start()

    table = v.weigh_out[sp]
    for k in range(1, count):
        weigh_copies[k - 1].wait_recv()
        table = table + v.weigh_in[k]
    filled = jnp.concatenate([table, jnp.zeros((LANES - lines, rows), single)], axis=0)
    v.weigh[...] = jnp.transpose(filled)
    for name in ("mixer", "stream", "gain"):
        loads[name].wait()

    carry = jnp.zeros((groups, LANES), single)
    for k in range(count - 1, 0, -1):
        end_copies[k - 1].wait_recv()
        longer = v.ends[k, 0:groups, :] * carry + v.ends[k, groups : 2 * groups, :]
        carry = jnp.where(sp >= k, longer, carry)
    carry = jnp.concatenate([carry[n : n + 1, :] for n in range(groups)], axis=1)
    order = [(1 - x, 1 - c), (x, 1 - c), (1 - x, c), (x, c)]
    for n, (chip, core) in enumerate(order):
        at = pl.ds(pl.multiple_of((chip * 2 + core) * kept, kept), kept)
        recurrent = v.state[at, :] + v.factor[at, :] * carry
        v.gated[n * kept : (n + 1) * kept, :] = (recurrent * v.gelu[at, :]).astype(kind)

    pieces = v.pair_send.shape[0]
    piece = width // pieces

    def pair(n):
        cols = pl.ds(n * piece, piece)
        return copy(
            v.give.at[:, :, cols], v.got.at[:, :, cols], v.pair_send.at[n], v.pair_recv.at[n],
            peer_c,
        )

    for n in range(pieces):
        cols = slice(n * piece, (n + 1) * piece)
        value = jnp.dot(v.gated[...], v.mixer[:, cols], preferred_element_type=single)
        v.give[:, :, cols] = value[: 2 * kept].astype(kind).reshape(2, kept, piece)
        v.keep[:, :, cols] = value[2 * kept :].reshape(2, kept, piece)
        pair(n).start()
    for n in range(pieces):
        pair(n).wait_recv()

    def part_of(h):
        return pl.ds(h * half, half)

    def cross(h):
        return copy(
            v.over.at[part_of(h)], v.came.at[part_of(h)], v.cross_send.at[h], v.cross_recv.at[h],
            peer_x,
        )

    for h in range(2):
        at = slice(h * half, (h + 1) * half)
        v.over[at, :] = (v.keep[0, at, :] + v.got[0, at, :].astype(single)).astype(kind)
        cross(h).start()

    xs, part = (v.xs, v.part)

    def ax(k, h):
        return copy(
            xs.at[k, 0, part_of(h)], xs.at[k, DX, part_of(h)], v.ax_send.at[k, h],
            v.ax_recv.at[k, h], peer_x,
        )

    def ay(k, h):
        return copy(
            xs.at[k, 0, part_of(h)], xs.at[k, DY, part_of(h)], v.ay_send.at[k, h],
            v.ay_recv.at[k, h], peer_y,
        )

    def fy(k):
        return copy(
            xs.at[k, DX, part_of(0)], xs.at[k, DX + DY, part_of(0)], v.af_send.at[k, 0],
            v.af_recv.at[k, 0], peer_y,
        )

    def fx(k):
        return copy(
            xs.at[k, DY, part_of(1)], xs.at[k, DX + DY, part_of(1)], v.af_send.at[k, 1],
            v.af_recv.at[k, 1], peer_x,
        )

    def ac(k, s):
        return copy(
            xs.at[k, s], xs.at[k, DC + s], v.ac_send.at[k, s], v.ac_recv.at[k, s], peer_c
        )

    def upward(i, h):
        return copy(
            xs.at[i - 1, 0, part_of(h)], xs.at[i, 0, part_of(h)], v.up_send.at[i, h],
            v.az_recv.at[i, h], plane(1),
        )

    def downward(i, h):
        return copy(
            xs.at[(depth - i + 1) % depth, 0, part_of(h)], xs.at[depth - i, 0, part_of(h)],
            v.dn_send.at[i, h], v.az_recv.at[depth - i, h], plane(depth - 1),
        )

    def landed(k, h):
        return copy(
            xs.at[0, 0, part_of(h)], xs.at[k, 0, part_of(h)], v.up_send.at[k, h],
            v.az_recv.at[k, h], plane(1),
        )

    for h in range(2):
        at = slice(h * half, (h + 1) * half)
        cross(h).wait_recv()
        total = v.keep[1, at, :] + v.got[1, at, :].astype(single) + v.came[at, :].astype(single)
        hidden = (v.stream[at, :].astype(single) + total).astype(kind)
        v.hidden[at, :] = hidden
        wide = hidden.astype(single)
        mean = jnp.mean(wide * wide, axis=-1, keepdims=True)
        normed = wide * lax.rsqrt(mean + NORM_EPSILON) * v.gain[...]
        xs[0, 0, at, :] = normed.astype(kind)
        ax(0, h).start()
        ay(0, h).start()

        @pl.when(z < depth - 1)
        def _():
            upward(1, h).start()

        @pl.when(z > 0)
        def _():
            downward(1, h).start()

    ac(0, 0).start()
    for name in ("gate_w", "up_w", "down_w"):
        loads[name].wait()

    def rc(k):
        return copy(
            part.at[k, pl.ds(DC, DC)], v.from_core.at[k], v.rc_send.at[k], v.rc_recv.at[k], peer_c
        )

    def rs(k, n):
        sems = (v.rs_send.at[k, n], v.rs_recv.at[k, n])
        if n == 0:
            return copy(part.at[k, DX + DY, part_of(0)], v.from_y.at[k, 1], *sems, peer_y)
        if n == 1:
            return copy(part.at[k, DX + DY, part_of(1)], v.from_x.at[k, 1], *sems, peer_x)
        if n == 2:
            return copy(part.at[k, DY, part_of(0)], v.from_y.at[k, 0], *sems, peer_y)
        if n == 3:
            return copy(part.at[k, DX, part_of(1)], v.from_x.at[k, 0], *sems, peer_x)
        if n == 4:
            return copy(part.at[k, DX, part_of(0)], v.last_x.at[k], *sems, peer_x)
        return copy(part.at[k, DY, part_of(1)], v.last_y.at[k], *sems, peer_y)

    def zr(k):
        return copy(
            part.at[k, 0], v.from_z.at[k], v.rz_send.at[k], v.rz_recv.at[k], plane(depth - k)
        )

    lane = lax.broadcasted_iota(jnp.int32, (kept, LANES), 1)

    def share_of(k, j):
        plane_from = (z + depth - k) % depth
        columns = []
        for s in range(DC):
            y_from = 1 - y if s & DY else y
            x_from = 1 - x if s & DX else x
            c_from = 1 - c if j else c
            at = pl.ds(pl.multiple_of((x_from * 2 + c_from) * kept, kept), kept)
            mine = lane == plane_from * 2 + y_from
            columns.append(
                jnp.sum(jnp.where(mine, v.weigh[at, :], 0.0), axis=1, keepdims=True)
            )
        return jnp.concatenate(columns, axis=0)

    def activated(k, j):
        rows_in = xs[k, j * DC : (j + 1) * DC].reshape(DC * kept, width)
        g = jnp.dot(rows_in, v.gate_w[...], preferred_element_type=single)
        u = jnp.dot(rows_in, v.up_w[...], preferred_element_type=single)
        return (clamp_units(g, u) * share_of(k, j)).astype(kind)

    def theirs(k):
        act = activated(k, 1)
        for n in range(pieces):
            cols = slice(n * piece, (n + 1) * piece)
            down = jnp.dot(act, v.down_w[:, cols], preferred_element_type=single)
            part[k, DC : 2 * DC, :, cols] = down.astype(kind).reshape(DC, kept, piece)
        rc(k).start()

    def ours(k):
        act = activated(k, 0)
        rc(k).wait_recv()
        for n in range(pieces):
            cols = slice(n * piece, (n + 1) * piece)
            down = jnp.dot(act, v.down_w[:, cols], preferred_element_type=single)
            down = down.reshape(DC, kept, piece) + v.from_core[k, :, :, cols].astype(single)
            part[k, 0:DC, :, cols] = down.astype(kind)

    def spread_first(k):
        ax(k, 0).wait_recv()
        fy(k).start()
        ay(k, 1).wait_recv()
        fx(k).start()

    def spread_rest(k):
        ax(k, 1).wait_recv()
        ac(k, DX).start()
        ay(k, 0).wait_recv()
        ac(k, DY).start()

    def spread_last(k):
        af_y, af_x = (fy(k), fx(k))
        af_y.wait_recv()
        af_x.wait_recv()
        ac(k, DX + DY).start()

    def enter(k):
        for h in range(2):
            landed(k, h).wait_recv()

        @pl.when((k <= z) & (z < depth - 1))
        def _():
            for h in range(2):
                upward(k + 1, h).start()

        @pl.when((k > z) & (z > 0))
        def _():
            for h in range(2):
                downward(depth - k + 1, h).start()

        ax(k, 0).start()
        ay(k, 1).start()
        ax(k, 1).start()
        ay(k, 0).start()
        ac(k, 0).start()

    def reduce_first(k):
        for n in range(4):
            rs(k, n).start()

    def reduce_next(k):
        rs(k, 0).wait_recv()
        now = part[k, DX, 0:half].astype(single) + v.from_y[k, 1].astype(single)
        part[k, DX, 0:half] = now.astype(kind)
        rs(k, 4).start()
        rs(k, 1).wait_recv()
        now = part[k, DY, half:kept].astype(single) + v.from_x[k, 1].astype(single)
        part[k, DY, half:kept] = now.astype(kind)
        rs(k, 5).start()

    def reduced(k):
        for n in (2, 3, 4, 5):
            rs(k, n).wait_recv()
        upper = part[k, 0, 0:half].astype(single) + v.from_y[k, 0].astype(single)
        lower = part[k, 0, half:kept].astype(single) + v.from_x[k, 0].astype(single)
        return (upper + v.last_x[k].astype(single), lower + v.last_y[k].astype(single))

    def reduce_last(k):
        upper, lower = reduced(k)
        part[k, 0, 0:half] = upper.astype(kind)
        part[k, 0, half:kept] = lower.astype(kind)
        zr(k).start()

    def step(q, none):
        k = nearest(z, q % depth, depth)
        k_next = nearest(z, (q + 1) % depth, depth)
        k_done = nearest(z, (q + depth - 1) % depth, depth)
        k_older = nearest(z, (q + depth - 2) % depth, depth)
        live, late = (q < depth, q > 0)

        @pl.when(live)
        def _():
            spread_first(k)

        @pl.when(late)
        def _():
            for s in range(DC):
                ac(k_done, s).wait_recv()
            theirs(k_done)

        @pl.when(q + 1 < depth)
        def _():
            enter(k_next)

        @pl.when(live)
        def _():
            spread_rest(k)

        @pl.when(q > 3)
        def _():
            reduce_next(k_older)

        @pl.when(late)
        def _():
            ours(k_done)

        @pl.when(q > 2)
        def _():
            reduce_first(k_done)

        @pl.when(live)
        def _():
            spread_last(k)

        return none

    lax.fori_loop(0, depth + 1, step, 0)
    k_1, k_near, k_far = [nearest(z, p, depth) for p in (1, depth - 2, depth - 1)]
    reduce_last(k_near)
    reduce_next(k_far)
    reduce_first(k_1)
    reduce_last(k_far)
    reduce_next(k_1)
    reduce_first(0)
    reduce_last(k_1)
    reduce_next(0)
    upper, lower = reduced(0)
    upper = upper + v.hidden[0:half, :].astype(single)
    lower = lower + v.hidden[half:kept, :].astype(single)
    for k in range(1, depth):
        zr(k).wait_recv()
        upper = upper + v.from_z[k, 0:half].astype(single)
        lower = lower + v.from_z[k, half:kept].astype(single)
    v.out[0:half, :] = upper.astype(v.out.dtype)
    v.out[half:kept, :] = lower.astype(v.out.dtype)

    for one in weigh_copies + end_copies:
        one.wait_send()
    for n in range(pieces):
        pair(n).wait_send()
    for h in range(2):
        cross(h).wait_send()

    def drain(k, none):
        for h in range(2):
            ax(k, h).wait_send()
            ay(k, h).wait_send()
        fy(k).wait_send()
        fx(k).wait_send()
        for s in range(DC):
            ac(k, s).wait_send()
        rc(k).wait_send()
        for n in range(6):
            rs(k, n).wait_send()
        return none

    lax.fori_loop(0, depth, drain, 0)

    def drain_planes(i, none):
        zr(i).wait_send()

        @pl.when((i - 1 <= z) & (z < depth - 1))
        def _():
            for h in range(2):
                upward(i, h).wait_send()

        @pl.when((z + i <= depth) & (z > 0))
        def _():
            for h in range(2):
                downward(i, h).wait_send()

        return none

    lax.fori_loop(1, depth, drain_planes, 0)


def layer(
    conv_input, gate_branch, conv_taps, narrow_maps, wide_maps, decay, decay_shift, mixer_out,
    stream, gain, routes, shares, expert_gate, expert_up, expert_down,
):
    count = lax.axis_size("sp")
    depth = count // 2
    rows, channels = conv_input.shape
    kept, width = stream.shape
    half = kept // 2
    pieces = 4
    lines = -(-count // SUBLANES) * SUBLANES
    single, kind = (jnp.float32, jnp.bfloat16)
    dma = pltpu.SemaphoreType.DMA
    inputs = dict(
        conv=conv_input, gate=gate_branch, taps=conv_taps, narrow=narrow_maps, wide=wide_maps,
        decay=decay, shift=decay_shift, mixer=mixer_out, stream=stream, gain=gain, routes=routes,
        shares=shares, gate_w=expert_gate, up_w=expert_up, down_w=expert_down,
    )
    scratch = {
        name: pltpu.VMEM(one.shape[1:] if name.endswith("_w") else one.shape, one.dtype)
        for name, one in inputs.items()
    }
    flat = pltpu.VMEM((rows, channels), single)
    scratch.update(
        soft=pltpu.VMEM(decay.shape, single),
        gelu=flat,
        head=pltpu.VMEM((SUBLANES, channels), single),
        halo=pltpu.VMEM((2 * SUBLANES, channels), kind),
        factor=flat,
        state=flat,
        padded=pltpu.VMEM((rows + SUBLANES, channels), single),
        log_keep=flat,
        drive_keep=flat,
        ends=pltpu.VMEM((count, 2 * channels // LANES, LANES), single),
        weigh_out=pltpu.VMEM((count, lines, rows), single),
        weigh_in=pltpu.VMEM((count, lines, rows), single),
        weigh=pltpu.VMEM((rows, LANES), single),
        gated=pltpu.VMEM((rows, channels), kind),
        give=pltpu.VMEM((2, kept, width), kind),
        got=pltpu.VMEM((2, kept, width), kind),
        keep=pltpu.VMEM((2, kept, width), single),
        over=pltpu.VMEM((kept, width), kind),
        came=pltpu.VMEM((kept, width), kind),
        hidden=pltpu.VMEM((kept, width), kind),
        xs=pltpu.VMEM((depth, 2 * DC, kept, width), kind),
        part=pltpu.VMEM((depth, 2 * DC, kept, width), kind),
        from_core=pltpu.VMEM((depth, DC, kept, width), kind),
        from_y=pltpu.VMEM((depth, 2, half, width), kind),
        from_x=pltpu.VMEM((depth, 2, half, width), kind),
        last_x=pltpu.VMEM((depth, half, width), kind),
        last_y=pltpu.VMEM((depth, half, width), kind),
        from_z=pltpu.VMEM((depth, kept, width), kind),
        load_sem=dma((len(inputs),)),
        halo_send=dma,
        halo_recv=dma,
    )
    for name, shape in dict(
        weigh=(count,), end=(count,), pair=(pieces,), cross=(2,), ax=(depth, 2), ay=(depth, 2),
        af=(depth, 2), ac=(depth, DC), rc=(depth,), rs=(depth, 6), rz=(depth,),
    ).items():
        scratch[name + "_send"] = dma(shape)
        scratch[name + "_recv"] = dma(shape)
    for name in ("up_send", "dn_send", "az_recv"):
        scratch[name] = dma((depth, 2))
    names = [name + "_hbm" for name in inputs] + ["out"] + list(scratch)
    return pl.pallas_call(
        functools.partial(layer_kernel, count, names),
        out_shape=jax.ShapeDtypeStruct((kept, width), kind),
        in_specs=[pl.BlockSpec(memory_space=pl.ANY)] * len(inputs),
        out_specs=pl.BlockSpec(memory_space=pltpu.VMEM),
        scratch_shapes=list(scratch.values()),
        compiler_params=pltpu.CompilerParams(
            collective_id=1, has_side_effects=True, vmem_limit_bytes=60 * 1024 * 1024
        ),
    )(*inputs.values())


def shards(
    conv_input,
    gate_branch,
    conv_taps,
    narrow_maps,
    wide_maps,
    decay_param,
    decay_shift,
    mixer_out,
    stream,
    norm_gain,
    routes,
    route_weights,
    expert_gate,
    expert_up,
    expert_down,
):
    seq_rows, channels = conv_input.shape
    tap_count = conv_taps.shape[0]
    tp_count = lax.axis_size("tp")
    tok_local = seq_rows // tp_count
    top_count = routes.shape[1]
    expert_total = expert_gate.shape[0] * lax.axis_size("sp")
    capacity = max(2, 2 * tok_local * top_count // expert_total)
    whole_rows = capacity >= tok_local and expert_gate.shape[0] == 1
    if whole_rows and tp_count == 4 and lax.axis_size("sp") == 8:
        return layer(
            conv_input, gate_branch, conv_taps, narrow_maps, wide_maps, decay_param[None, :],
            decay_shift, mixer_out, stream, norm_gain[None, :], routes.T, route_weights.T,
            expert_gate, expert_up, expert_down,
        )
    own_index = lax.axis_index("tp")
    own_rows = lax.dynamic_slice_in_dim(routes, own_index * tok_local, tok_local, 0)
    own_weights = lax.dynamic_slice_in_dim(route_weights, own_index * tok_local, tok_local, 0)
    soft = jax.nn.softplus(-decay_param)[None, :]
    earlier = shifted(conv_input[seq_rows - tap_count + 1 :], "sp", 1)
    head = jnp.zeros((SUBLANES, channels), jnp.float32)
    head = head.at[SUBLANES - tap_count + 1 :].set(earlier.astype(jnp.float32))
    factors, local_state = mix_local(
        head, conv_input, conv_taps, narrow_maps, wide_maps, soft, decay_shift
    )
    ends = lax.all_gather(jnp.stack([factors[-1], local_state[-1]]), "sp")
    mine = lax.axis_index("sp")
    state = jnp.zeros((channels,), jnp.float32)
    for position in range(lax.axis_size("sp") - 1):
        longer = ends[position, 0] * state + ends[position, 1]
        state = jnp.where(position < mine, longer, state)
    carried = (None, state)
    recurrent = local_state + factors * carried[1]
    gated_rows = (recurrent * jax.nn.gelu(gate_branch.astype(jnp.float32))).astype(jnp.bfloat16)
    mixer_sum = lax.psum_scatter(
        jnp.dot(gated_rows, mixer_out, preferred_element_type=jnp.float32).astype(jnp.bfloat16),
        "tp",
        scatter_dimension=0,
        tiled=True,
    ).astype(jnp.float32)
    hidden_f = stream.astype(jnp.float32) + mixer_sum
    hidden = hidden_f.astype(jnp.bfloat16)
    hidden_f = hidden.astype(jnp.float32)
    normed = (
        hidden_f
        * lax.rsqrt(jnp.mean(hidden_f * hidden_f, axis=-1, keepdims=True) + NORM_EPSILON)
        * norm_gain
    ).astype(jnp.bfloat16)
    model_width = normed.shape[1]
    assignments = tok_local * top_count
    own_routes = own_rows.reshape(assignments)
    own_ranks = slot_ranks(own_routes[None, :], expert_total)[0]
    source = jnp.arange(assignments, dtype=jnp.int32) // top_count
    slot_source = (
        jnp.full((expert_total * capacity,), -1, jnp.int32)
        .at[own_routes * capacity + own_ranks]
        .set(source)
    )
    outgoing = take_rows(normed, slot_source).reshape(expert_total, 1, capacity, model_width)
    partial_value = expert_work(
        lax.all_gather(
            lax.all_to_all(outgoing, "sp", split_axis=0, concat_axis=0, tiled=True),
            "tp",
            axis=1,
            tiled=True,
        ),
        expert_gate,
        expert_up,
        expert_down,
    )
    summed = lax.psum_scatter(
        partial_value.astype(jnp.bfloat16), "tp", scatter_dimension=1, tiled=True
    )
    returned = lax.all_to_all(summed, "sp", split_axis=0, concat_axis=0, tiled=True)
    own_slots = own_routes * capacity + own_ranks
    picked = returned.reshape(expert_total * capacity, model_width)[own_slots]
    combined = jnp.sum(
        picked.reshape(tok_local, top_count, model_width).astype(jnp.float32)
        * own_weights[:, :, None],
        axis=1,
    )
    return (hidden_f + combined).astype(jnp.bfloat16)


def solution(mesh):
    placed = (
        P("sp", "tp"),
        P("sp", "tp"),
        P(None, "tp"),
        P(None, "tp", None, None),
        P(None, "tp", None, None),
        P("tp"),
        P("sp", "tp"),
        P("tp", None),
        P(("sp", "tp"), None),
        P(),
        P("sp", None),
        P("sp", None),
        P("sp", None, "tp"),
        P("sp", None, "tp"),
        P("sp", "tp", None),
    )
    return jax.shard_map(
        shards, mesh=mesh, in_specs=placed, out_specs=P(("sp", "tp"), None), check_vma=False
    )
```

time: 140 us -> 106 us (0.76)
  Pallas kernels: 125 us -> 104 us
  local copies, waits for them, and re-layouts: 12.6 us -> 1.67 us
    pallas_call x2 -> x1, Pallas kernels: 125 us -> 104 us  [layer(): pl.pallas_call(functools.partial(layer_kernel, count, names), out_shape=j...]
    unnamed x25 -> x1, local copies, waits for them, and re-layouts: 11.8 us -> 1.67 us
where the time goes in v1:
time: 106 us
  Pallas kernels  104 us (98%)
  local copies, waits for them, and re-layouts  1.67 us (2%)
    pallas_call x1, Pallas kernels, layer(): pl.pallas_call(functools.partial(layer_kernel, count, names), out_shape=j...  104 us

profile of v1, /device:TPU:0, one launch (start us, length us, event | category | flops | bytes accessed | tf_op | source)
XLA Modules:
  0.0 105.7 jit_solution(5021922496870224265)
XLA Ops:
  0.0 104.0 %shard_map.145 = bf16[64,2048]{1,0:T(8,128)(2,1)} custom-call(bf16[256,512]{1,0:T(8,128)(2,1)} %refs_0_.1, bf16[256,512]{1,0:T(8,128)(2,1)} %refs_1_.1, f32[4,512]{1,0:T(4,128)} %refs_2_.1, bf16[2,2,128,128]{3,2,1,0:T(8,128)(2,1)} %refs_3_.1, bf16[2,1,256,256]{3,2,1,0:T(8,128)(2,1)} %refs_4_.1, f32[1,512]{1,0:T(1,128)} %bitcast.7, f32[256,512]{1,0:T(8,128)} %refs_6_.1, ...), custom_call_target="tpu_custom_call" | custom-call | tf_op jit(solution)/shard_map/pallas_call | solution.py:682
  104.0 1.7 %copy.17 = bf16[64,2048]{1,0:T(8,128)(2,1)} copy(bf16[64,2048]{1,0:T(8,128)(2,1)} %shard_map.145) | data formatting | bytes 524288

commit v2 on v1

--- a/solution.py
+++ b/solution.py
@@ -183,6 +183,9 @@
             device_id=peer, device_id_type=mesh_id,
         )
 
+    def all_of(ref, sem):
+        return copy(ref, ref, sem, sem, peer_c)
+
     barrier = pltpu.get_barrier_semaphore()
     peers = [peer_x, peer_c] + [later(k) for k in range(1, count)]
     for peer in peers:
@@ -219,8 +222,8 @@
         v.weigh_out[e] = jnp.where(line == sp, share, 0.0)
     weigh_copies = [
         copy(
-            v.weigh_out.at[(sp + k) % count], v.weigh_in.at[k], v.weigh_send.at[k],
-            v.weigh_recv.at[k], later(k),
+            v.weigh_out.at[(sp + k) % count], v.weigh_in.at[k], v.weigh_send, v.weigh_recv,
+            later(k),
         )
         for k in range(1, count)
     ]
@@ -249,24 +252,25 @@
         v.ends[0, n : n + 1, :] = v.factor[rows - 1 : rows, cols]
         v.ends[0, groups + n : groups + n + 1, :] = v.state[rows - 1 : rows, cols]
     end_copies = [
-        copy(v.ends.at[0], v.ends.at[k], v.end_send.at[k], v.end_recv.at[k], later(k))
+        copy(v.ends.at[0], v.ends.at[k], v.end_send, v.end_recv, later(k))
         for k in range(1, count)
     ]
     for one in end_copies:
         one.start()
 
+    others = pl.ds(1, count - 1)
+    all_of(v.weigh_in.at[others], v.weigh_recv).wait_recv()
     table = v.weigh_out[sp]
     for k in range(1, count):
-        weigh_copies[k - 1].wait_recv()
         table = table + v.weigh_in[k]
     filled = jnp.concatenate([table, jnp.zeros((LANES - lines, rows), single)], axis=0)
     v.weigh[...] = jnp.transpose(filled)
     for name in ("mixer", "stream", "gain"):
         loads[name].wait()
 
+    all_of(v.ends.at[others], v.end_recv).wait_recv()
     carry = jnp.zeros((groups, LANES), single)
     for k in range(count - 1, 0, -1):
-        end_copies[k - 1].wait_recv()
         longer = v.ends[k, 0:groups, :] * carry + v.ends[k, groups : 2 * groups, :]
         carry = jnp.where(sp >= k, longer, carry)
     carry = jnp.concatenate([carry[n : n + 1, :] for n in range(groups)], axis=1)
@@ -276,14 +280,13 @@
         recurrent = v.state[at, :] + v.factor[at, :] * carry
         v.gated[n * kept : (n + 1) * kept, :] = (recurrent * v.gelu[at, :]).astype(kind)
 
-    pieces = v.pair_send.shape[0]
+    pieces = 4
     piece = width // pieces
 
     def pair(n):
         cols = pl.ds(n * piece, piece)
         return copy(
-            v.give.at[:, :, cols], v.got.at[:, :, cols], v.pair_send.at[n], v.pair_recv.at[n],
-            peer_c,
+            v.give.at[:, :, cols], v.got.at[:, :, cols], v.pair_send, v.pair_recv, peer_c
         )
 
     for n in range(pieces):
@@ -292,15 +295,14 @@
         v.give[:, :, cols] = value[: 2 * kept].astype(kind).reshape(2, kept, piece)
         v.keep[:, :, cols] = value[2 * kept :].reshape(2, kept, piece)
         pair(n).start()
-    for n in range(pieces):
-        pair(n).wait_recv()
+    all_of(v.got, v.pair_recv).wait_recv()
 
     def part_of(h):
         return pl.ds(h * half, half)
 
     def cross(h):
         return copy(
-            v.over.at[part_of(h)], v.came.at[part_of(h)], v.cross_send.at[h], v.cross_recv.at[h],
+            v.over.at[part_of(h)], v.came.at[part_of(h)], v.cross_send, v.cross_recv.at[h],
             peer_x,
         )
 
@@ -313,50 +315,48 @@
 
     def ax(k, h):
         return copy(
-            xs.at[k, 0, part_of(h)], xs.at[k, DX, part_of(h)], v.ax_send.at[k, h],
+            xs.at[k, 0, part_of(h)], xs.at[k, DX, part_of(h)], v.ax_send,
             v.ax_recv.at[k, h], peer_x,
         )
 
     def ay(k, h):
         return copy(
-            xs.at[k, 0, part_of(h)], xs.at[k, DY, part_of(h)], v.ay_send.at[k, h],
+            xs.at[k, 0, part_of(h)], xs.at[k, DY, part_of(h)], v.ay_send,
             v.ay_recv.at[k, h], peer_y,
         )
 
     def fy(k):
         return copy(
-            xs.at[k, DX, part_of(0)], xs.at[k, DX + DY, part_of(0)], v.af_send.at[k, 0],
-            v.af_recv.at[k, 0], peer_y,
+            xs.at[k, DX, part_of(0)], xs.at[k, DX + DY, part_of(0)], v.af_send,
+            v.af_recv.at[k], peer_y,
         )
 
     def fx(k):
         return copy(
-            xs.at[k, DY, part_of(1)], xs.at[k, DX + DY, part_of(1)], v.af_send.at[k, 1],
-            v.af_recv.at[k, 1], peer_x,
+            xs.at[k, DY, part_of(1)], xs.at[k, DX + DY, part_of(1)], v.af_send,
+            v.af_recv.at[k], peer_x,
         )
 
     def ac(k, s):
         return copy(
-            xs.at[k, s], xs.at[k, DC + s], v.ac_send.at[k, s], v.ac_recv.at[k, s], peer_c
-        )
-
-    def upward(i, h):
-        return copy(
-            xs.at[i - 1, 0, part_of(h)], xs.at[i, 0, part_of(h)], v.up_send.at[i, h],
-            v.az_recv.at[i, h], plane(1),
-        )
-
-    def downward(i, h):
-        return copy(
-            xs.at[(depth - i + 1) % depth, 0, part_of(h)], xs.at[depth - i, 0, part_of(h)],
-            v.dn_send.at[i, h], v.az_recv.at[depth - i, h], plane(depth - 1),
-        )
-
-    def landed(k, h):
-        return copy(
-            xs.at[0, 0, part_of(h)], xs.at[k, 0, part_of(h)], v.up_send.at[k, h],
-            v.az_recv.at[k, h], plane(1),
-        )
+            xs.at[k, s], xs.at[k, DC + s], v.ac_send, v.ac_recv.at[k], peer_c
+        )
+
+    whole = pl.ds(0, kept)
+
+    def upward(i, at):
+        return copy(
+            xs.at[i - 1, 0, at], xs.at[i, 0, at], v.up_send.at[i], v.az_recv.at[i], plane(1)
+        )
+
+    def downward(i, at):
+        return copy(
+            xs.at[(depth - i + 1) % depth, 0, at], xs.at[depth - i, 0, at], v.dn_send.at[i],
+            v.az_recv.at[depth - i], plane(depth - 1),
+        )
+
+    def landed(k):
+        return all_of(xs.at[k, 0], v.az_recv.at[k])
 
     for h in range(2):
         at = slice(h * half, (h + 1) * half)
@@ -373,11 +373,11 @@
 
         @pl.when(z < depth - 1)
         def _():
-            upward(1, h).start()
+            upward(1, part_of(h)).start()
 
         @pl.when(z > 0)
         def _():
-            downward(1, h).start()
+            downward(1, part_of(h)).start()
 
     ac(0, 0).start()
     for name in ("gate_w", "up_w", "down_w"):
@@ -385,26 +385,26 @@
 
     def rc(k):
         return copy(
-            part.at[k, pl.ds(DC, DC)], v.from_core.at[k], v.rc_send.at[k], v.rc_recv.at[k], peer_c
+            part.at[k, pl.ds(DC, DC)], v.from_core.at[k], v.rc_send, v.rc_recv.at[k], peer_c
         )
 
     def rs(k, n):
-        sems = (v.rs_send.at[k, n], v.rs_recv.at[k, n])
+        sems = (v.rs_send, v.rs_recv.at[k, min(n, 2)])
         if n == 0:
-            return copy(part.at[k, DX + DY, part_of(0)], v.from_y.at[k, 1], *sems, peer_y)
+            return copy(part.at[k, DX + DY, part_of(0)], v.first.at[k, 0], *sems, peer_y)
         if n == 1:
-            return copy(part.at[k, DX + DY, part_of(1)], v.from_x.at[k, 1], *sems, peer_x)
+            return copy(part.at[k, DX + DY, part_of(1)], v.first.at[k, 1], *sems, peer_x)
         if n == 2:
-            return copy(part.at[k, DY, part_of(0)], v.from_y.at[k, 0], *sems, peer_y)
+            return copy(part.at[k, DY, part_of(0)], v.rest.at[k, 0], *sems, peer_y)
         if n == 3:
-            return copy(part.at[k, DX, part_of(1)], v.from_x.at[k, 0], *sems, peer_x)
+            return copy(part.at[k, DX, part_of(1)], v.rest.at[k, 1], *sems, peer_x)
         if n == 4:
-            return copy(part.at[k, DX, part_of(0)], v.last_x.at[k], *sems, peer_x)
-        return copy(part.at[k, DY, part_of(1)], v.last_y.at[k], *sems, peer_y)
+            return copy(part.at[k, DX, part_of(0)], v.rest.at[k, 2], *sems, peer_x)
+        return copy(part.at[k, DY, part_of(1)], v.rest.at[k, 3], *sems, peer_y)
 
     def zr(k):
         return copy(
-            part.at[k, 0], v.from_z.at[k], v.rz_send.at[k], v.rz_recv.at[k], plane(depth - k)
+            part.at[k, 0], v.from_z.at[k], v.rz_send, v.rz_recv, plane(depth - k)
         )
 
     lane = lax.broadcasted_iota(jnp.int32, (kept, LANES), 1)
@@ -459,25 +459,27 @@
         ac(k, DY).start()
 
     def spread_last(k):
-        af_y, af_x = (fy(k), fx(k))
-        af_y.wait_recv()
-        af_x.wait_recv()
+        all_of(xs.at[k, DX + DY], v.af_recv.at[k]).wait_recv()
         ac(k, DX + DY).start()
 
+    def relay(i):
+        @pl.when(i <= z)
+        def _():
+            landed(i).wait_recv()
+
+            @pl.when(z < depth - 1)
+            def _():
+                upward(i + 1, whole).start()
+
+        @pl.when(z + i < depth)
+        def _():
+            landed(depth - i).wait_recv()
+
+            @pl.when(z > 0)
+            def _():
+                downward(i + 1, whole).start()
+
     def enter(k):
-        for h in range(2):
-            landed(k, h).wait_recv()
-
-        @pl.when((k <= z) & (z < depth - 1))
-        def _():
-            for h in range(2):
-                upward(k + 1, h).start()
-
-        @pl.when((k > z) & (z > 0))
-        def _():
-            for h in range(2):
-                downward(depth - k + 1, h).start()
-
         ax(k, 0).start()
         ay(k, 1).start()
         ax(k, 1).start()
@@ -490,20 +492,19 @@
 
     def reduce_next(k):
         rs(k, 0).wait_recv()
-        now = part[k, DX, 0:half].astype(single) + v.from_y[k, 1].astype(single)
+        now = part[k, DX, 0:half].astype(single) + v.first[k, 0].astype(single)
         part[k, DX, 0:half] = now.astype(kind)
         rs(k, 4).start()
         rs(k, 1).wait_recv()
-        now = part[k, DY, half:kept].astype(single) + v.from_x[k, 1].astype(single)
+        now = part[k, DY, half:kept].astype(single) + v.first[k, 1].astype(single)
         part[k, DY, half:kept] = now.astype(kind)
         rs(k, 5).start()
 
     def reduced(k):
-        for n in (2, 3, 4, 5):
-            rs(k, n).wait_recv()
-        upper = part[k, 0, 0:half].astype(single) + v.from_y[k, 0].astype(single)
-        lower = part[k, 0, half:kept].astype(single) + v.from_x[k, 0].astype(single)
-        return (upper + v.last_x[k].astype(single), lower + v.last_y[k].astype(single))
+        all_of(v.rest.at[k], v.rs_recv.at[k, 2]).wait_recv()
+        upper = part[k, 0, 0:half].astype(single) + v.rest[k, 0].astype(single)
+        lower = part[k, 0, half:kept].astype(single) + v.rest[k, 1].astype(single)
+        return (upper + v.rest[k, 2].astype(single), lower + v.rest[k, 3].astype(single))
 
     def reduce_last(k):
         upper, lower = reduced(k)
@@ -524,12 +525,12 @@
 
         @pl.when(late)
         def _():
-            for s in range(DC):
-                ac(k_done, s).wait_recv()
+            all_of(xs.at[k_done, pl.ds(DC, DC)], v.ac_recv.at[k_done]).wait_recv()
             theirs(k_done)
 
         @pl.when(q + 1 < depth)
         def _():
+            relay(q + 1)
             enter(k_next)
 
         @pl.when(live)
@@ -567,51 +568,43 @@
     upper, lower = reduced(0)
     upper = upper + v.hidden[0:half, :].astype(single)
     lower = lower + v.hidden[half:kept, :].astype(single)
+    beyond = pl.ds(1, depth - 1)
+    all_of(v.from_z.at[beyond], v.rz_recv).wait_recv()
     for k in range(1, depth):
-        zr(k).wait_recv()
         upper = upper + v.from_z[k, 0:half].astype(single)
         lower = lower + v.from_z[k, half:kept].astype(single)
-    v.out[0:half, :] = upper.astype(v.out.dtype)
-    v.out[half:kept, :] = lower.astype(v.out.dtype)
-
-    for one in weigh_copies + end_copies:
-        one.wait_send()
-    for n in range(pieces):
-        pair(n).wait_send()
-    for h in range(2):
-        cross(h).wait_send()
-
-    def drain(k, none):
-        for h in range(2):
-            ax(k, h).wait_send()
-            ay(k, h).wait_send()
-        fy(k).wait_send()
-        fx(k).wait_send()
-        for s in range(DC):
-            ac(k, s).wait_send()
-        rc(k).wait_send()
-        for n in range(6):
-            rs(k, n).wait_send()
-        return none
-
-    lax.fori_loop(0, depth, drain, 0)
-
-    def drain_planes(i, none):
-        zr(i).wait_send()
+    results = []
+    for h, value in enumerate((upper, lower)):
+        v.result[h * half : (h + 1) * half, :] = value.astype(v.result.dtype)
+        results.append(
+            pltpu.make_async_copy(
+                v.result.at[part_of(h)], v.out.at[part_of(h)], v.result_sem.at[h]
+            )
+        )
+        results[h].start()
+
+    every = pl.ds(0, depth)
+    quarter = xs.at[every, pl.ds(0, 1)]
+    for ref, sem in (
+        (v.weigh_in.at[others], v.weigh_send), (v.ends.at[others], v.end_send),
+        (v.give, v.pair_send), (v.over, v.cross_send), (quarter, v.ax_send),
+        (quarter, v.ay_send), (quarter, v.af_send), (xs.at[every, pl.ds(0, DC)], v.ac_send),
+        (part.at[every, pl.ds(DC, DC)], v.rc_send), (part.at[every, pl.ds(0, 3)], v.rs_send),
+        (v.from_z.at[beyond], v.rz_send),
+    ):
+        all_of(ref, sem).wait_send()
+    for i in range(1, depth):
 
         @pl.when((i - 1 <= z) & (z < depth - 1))
         def _():
-            for h in range(2):
-                upward(i, h).wait_send()
+            upward(i, whole).wait_send()
 
         @pl.when((z + i <= depth) & (z > 0))
         def _():
-            for h in range(2):
-                downward(i, h).wait_send()
-
-        return none
-
-    lax.fori_loop(1, depth, drain_planes, 0)
+            downward(i, whole).wait_send()
+
+    for one in results:
+        one.wait()
 
 
 def layer(
@@ -661,29 +654,29 @@
         xs=pltpu.VMEM((depth, 2 * DC, kept, width), kind),
         part=pltpu.VMEM((depth, 2 * DC, kept, width), kind),
         from_core=pltpu.VMEM((depth, DC, kept, width), kind),
-        from_y=pltpu.VMEM((depth, 2, half, width), kind),
-        from_x=pltpu.VMEM((depth, 2, half, width), kind),
-        last_x=pltpu.VMEM((depth, half, width), kind),
-        last_y=pltpu.VMEM((depth, half, width), kind),
+        first=pltpu.VMEM((depth, 2, half, width), kind),
+        rest=pltpu.VMEM((depth, 4, half, width), kind),
         from_z=pltpu.VMEM((depth, kept, width), kind),
+        result=pltpu.VMEM((kept, width), kind),
         load_sem=dma((len(inputs),)),
+        result_sem=dma((2,)),
         halo_send=dma,
         halo_recv=dma,
     )
-    for name, shape in dict(
-        weigh=(count,), end=(count,), pair=(pieces,), cross=(2,), ax=(depth, 2), ay=(depth, 2),
-        af=(depth, 2), ac=(depth, DC), rc=(depth,), rs=(depth, 6), rz=(depth,),
-    ).items():
-        scratch[name + "_send"] = dma(shape)
-        scratch[name + "_recv"] = dma(shape)
-    for name in ("up_send", "dn_send", "az_recv"):
-        scratch[name] = dma((depth, 2))
+    sent = ("weigh", "end", "pair", "cross", "ax", "ay", "af", "ac", "rc", "rs", "rz")
+    scratch.update({name + "_send": dma for name in sent})
+    landing = dict(
+        weigh=(), end=(), pair=(), cross=(2,), ax=(depth, 2), ay=(depth, 2), af=(depth,),
+        ac=(depth,), rc=(depth,), rs=(depth, 3), rz=(), az=(depth,),
+    )
+    scratch.update({name + "_recv": dma(shape) if shape else dma for name, shape in landing.items()})
+    scratch.update(up_send=dma((depth,)), dn_send=dma((depth,)))
     names = [name + "_hbm" for name in inputs] + ["out"] + list(scratch)
     return pl.pallas_call(
         functools.partial(layer_kernel, count, names),
         out_shape=jax.ShapeDtypeStruct((kept, width), kind),
         in_specs=[pl.BlockSpec(memory_space=pl.ANY)] * len(inputs),
-        out_specs=pl.BlockSpec(memory_space=pltpu.VMEM),
+        out_specs=pl.BlockSpec(memory_space=pl.ANY),
         scratch_shapes=list(scratch.values()),
         compiler_params=pltpu.CompilerParams(
             collective_id=1, has_side_effects=True, vmem_limit_bytes=60 * 1024 * 1024

time: 106 us -> 99.4 us (0.938)
  Pallas kernels: 104 us -> 97.6 us
    pallas_call x1, Pallas kernels: 104 us -> 97.6 us  [layer(): pl.pallas_call(functools.partial(layer_kernel, count, names), out_shape=j...]
where the time goes in v2:
time: 99.4 us; the launch traced here: 99.2 us
  Pallas kernels  97.6 us (98%)
  local copies, waits for them, and re-layouts  1.67 us (2%)
    pallas_call x1, Pallas kernels, layer(): pl.pallas_call(functools.partial(layer_kernel, count, names), out_shape=j...  97.6 us

profile of v2, /device:TPU:0, one launch (start us, length us, event | category | flops | bytes accessed | tf_op | source)
XLA Modules:
  0.0 99.2 jit_solution(2439186121826788754)
XLA Ops:
  0.0 97.6 %shard_map.145 = bf16[64,2048]{1,0:T(8,128)(2,1)} custom-call(bf16[256,512]{1,0:T(8,128)(2,1)} %refs_0_.1, bf16[256,512]{1,0:T(8,128)(2,1)} %refs_1_.1, f32[4,512]{1,0:T(4,128)} %refs_2_.1, bf16[2,2,128,128]{3,2,1,0:T(8,128)(2,1)} %refs_3_.1, bf16[2,1,256,256]{3,2,1,0:T(8,128)(2,1)} %refs_4_.1, f32[1,512]{1,0:T(1,128)} %bitcast.7, f32[256,512]{1,0:T(8,128)} %refs_6_.1, ...), custom_call_target="tpu_custom_call" | custom-call | tf_op jit(solution)/shard_map/pallas_call | solution.py:675
  97.6 1.7 %copy.17 = bf16[64,2048]{1,0:T(8,128)(2,1)} copy(bf16[64,2048]{1,0:T(8,128)(2,1)} %shard_map.145) | data formatting | bytes 524288

commit v3 on v2

--- a/solution.py
+++ b/solution.py
@@ -148,12 +148,8 @@
     )(head, conv_input, conv_taps, narrow_maps, wide_maps, soft, decay_shift)
 
 
-def nearest(z, p, depth):
-    short = jnp.minimum(z, depth - 1 - z)
-    near = p <= 2 * short
-    distance = jnp.where(near, (p + 1) // 2, p - short)
-    left = jnp.where(near, p % 2, jnp.where(z > depth - 1 - z, 1, 0))
-    return jnp.where(p == 0, 0, jnp.where(left == 1, distance, depth - distance))
+def turn(z, p, depth):
+    return jnp.where(p == 0, 0, jnp.where(z % 2 == 1, p, depth - p))
 
 
 def layer_kernel(count, names, *refs):
@@ -208,6 +204,94 @@
         v.conv.at[pl.ds(rows - halo_rows, halo_rows)], v.halo, v.halo_send, v.halo_recv, later(1)
     )
     halo_copy.start()
+
+    loads["decay"].wait()
+    t = jnp.exp(-v.decay[...])
+    v.soft[...] = t * (1.0 - t * (0.5 - t * (1.0 / 3.0 - t * (0.25 - t * (0.2 - t * (1.0 / 6.0))))))
+    for name in ("taps", "narrow", "wide", "shift"):
+        loads[name].wait()
+    taps = v.taps.shape[0]
+    lead = 2 * SUBLANES
+    v.padded[SUBLANES:, :] = v.conv[...].astype(single)
+    row_id = lax.broadcasted_iota(jnp.int32, (SUBLANES, channels), 0)
+
+    def drive(first, last):
+        at = slice(first, last)
+        total = jnp.zeros((last - first, channels), single)
+        for k in range(taps):
+            shift = SUBLANES - taps + 1 + k
+            total = total + v.padded[first + shift : last + shift, :] * v.taps[k : k + 1, :]
+        convolved = total.astype(kind)
+        narrow_size, wide_size = (v.narrow.shape[2], v.wide.shape[2])
+        spans = []
+        for j in range(v.wide.shape[1]):
+            base = j * (2 * narrow_size + wide_size)
+            spans.append((base, narrow_size, v.narrow, 2 * j))
+            spans.append((base + narrow_size, narrow_size, v.narrow, 2 * j + 1))
+            spans.append((base + 2 * narrow_size, wide_size, v.wide, j))
+        for start, size, maps, head in spans:
+            cols = slice(start, start + size)
+            piece = convolved[:, cols]
+            decay_pre = jnp.dot(piece, maps[0, head], preferred_element_type=single)
+            input_pre = jnp.dot(piece, maps[1, head], preferred_element_type=single)
+            log_decay = (
+                -DECAY_SCALE * jax.nn.sigmoid(decay_pre) * v.soft[:, cols] + v.shift[at, cols]
+            )
+            decay = jnp.exp(log_decay)
+            y2 = 2.0 * log_decay
+            series = -y2 * (
+                1.0 + y2 * (0.5 + y2 * (1.0 / 6.0 + y2 * (1.0 / 24.0 + y2 * (1.0 / 120.0))))
+            )
+            lost = jnp.where(y2 > -SERIES_LIMIT, series, 1.0 - decay * decay)
+            v.log_keep[at, cols] = decay
+            v.drive_keep[at, cols] = (
+                jnp.sqrt(lost) * jax.nn.sigmoid(input_pre) * piece.astype(single)
+            )
+
+    def tile(i, carried):
+        product, state = carried
+        at = pl.ds(pl.multiple_of(i * SUBLANES, SUBLANES), SUBLANES)
+        a, b = (v.log_keep[at, :], v.drive_keep[at, :])
+        hop = 1
+        while hop < SUBLANES:
+            inside = row_id >= hop
+            a_before = jnp.where(inside, pltpu.roll(a, hop, 0), 1.0)
+            b_before = jnp.where(inside, pltpu.roll(b, hop, 0), 0.0)
+            b = a * b_before + b
+            a = a * a_before
+            hop *= 2
+        b = b + a * state
+        a = a * product
+        v.factor[at, :] = a
+        v.state[at, :] = b
+        last = slice(SUBLANES - 1, SUBLANES)
+        return (a[last, :], b[last, :])
+
+    def scan(first, last):
+        start = (jnp.ones((1, channels), single), jnp.zeros((1, channels), single))
+        return lax.fori_loop(first // SUBLANES, last // SUBLANES, tile, start, unroll=2)
+
+    drive(lead, rows)
+    scan(lead, rows)
+    halo_copy.wait()
+    before = v.halo[...].astype(single)[halo_rows - SUBLANES :]
+    v.padded[0:SUBLANES, :] = jnp.where(sp > 0, before, jnp.zeros_like(before))
+    drive(0, lead)
+    lead_factor, lead_state = scan(0, lead)
+    rest_factor, rest_state = (v.factor[rows - 1 : rows, :], v.state[rows - 1 : rows, :])
+    end_factor = rest_factor * lead_factor
+    end_state = rest_state + rest_factor * lead_state
+    groups = channels // LANES
+    for n in range(groups):
+        cols = slice(n * LANES, (n + 1) * LANES)
+        v.ends[0, n : n + 1, :] = end_factor[:, cols]
+        v.ends[0, groups + n : groups + n + 1, :] = end_state[:, cols]
+    end_copies = [
+        copy(v.ends.at[0], v.ends.at[k], v.end_send, v.end_recv, later(k))
+        for k in range(1, count)
+    ]
+    for one in end_copies:
+        one.start()
 
     loads["routes"].wait()
     loads["shares"].wait()
@@ -230,54 +314,27 @@
     for one in weigh_copies:
         one.start()
 
-    loads["decay"].wait()
-    t = jnp.exp(-v.decay[...])
-    v.soft[...] = t * (1.0 - t * (0.5 - t * (1.0 / 3.0 - t * (0.25 - t * (0.2 - t * (1.0 / 6.0))))))
     loads["gate"].wait()
     g = v.gate[...].astype(single)
     v.gelu[...] = 0.5 * g * (1.0 + jnp.tanh(GELU_SCALE * (g + GELU_CUBIC * g * g * g)))
-    for name in ("taps", "narrow", "wide", "shift"):
-        loads[name].wait()
-
-    halo_copy.wait()
-    before = v.halo[...].astype(single)[halo_rows - SUBLANES :]
-    v.head[...] = jnp.where(sp > 0, before, jnp.zeros_like(before))
-    mix_kernel(
-        v.head, v.conv, v.taps, v.narrow, v.wide, v.soft, v.shift,
-        v.factor, v.state, v.padded, v.log_keep, v.drive_keep,
-    )
-    groups = channels // LANES
-    for n in range(groups):
-        cols = slice(n * LANES, (n + 1) * LANES)
-        v.ends[0, n : n + 1, :] = v.factor[rows - 1 : rows, cols]
-        v.ends[0, groups + n : groups + n + 1, :] = v.state[rows - 1 : rows, cols]
-    end_copies = [
-        copy(v.ends.at[0], v.ends.at[k], v.end_send, v.end_recv, later(k))
-        for k in range(1, count)
-    ]
-    for one in end_copies:
-        one.start()
-
-    others = pl.ds(1, count - 1)
-    all_of(v.weigh_in.at[others], v.weigh_recv).wait_recv()
-    table = v.weigh_out[sp]
-    for k in range(1, count):
-        table = table + v.weigh_in[k]
-    filled = jnp.concatenate([table, jnp.zeros((LANES - lines, rows), single)], axis=0)
-    v.weigh[...] = jnp.transpose(filled)
     for name in ("mixer", "stream", "gain"):
         loads[name].wait()
 
+    others = pl.ds(1, count - 1)
     all_of(v.ends.at[others], v.end_recv).wait_recv()
     carry = jnp.zeros((groups, LANES), single)
     for k in range(count - 1, 0, -1):
         longer = v.ends[k, 0:groups, :] * carry + v.ends[k, groups : 2 * groups, :]
         carry = jnp.where(sp >= k, longer, carry)
     carry = jnp.concatenate([carry[n : n + 1, :] for n in range(groups)], axis=1)
+    beyond_lead = lead_state + lead_factor * carry
+    row = lax.broadcasted_iota(jnp.int32, (kept, channels), 0)
     order = [(1 - x, 1 - c), (x, 1 - c), (1 - x, c), (x, c)]
     for n, (chip, core) in enumerate(order):
-        at = pl.ds(pl.multiple_of((chip * 2 + core) * kept, kept), kept)
-        recurrent = v.state[at, :] + v.factor[at, :] * carry
+        first = (chip * 2 + core) * kept
+        at = pl.ds(pl.multiple_of(first, kept), kept)
+        entering = jnp.where(row + first < lead, carry, beyond_lead)
+        recurrent = v.state[at, :] + v.factor[at, :] * entering
         v.gated[n * kept : (n + 1) * kept, :] = (recurrent * v.gelu[at, :]).astype(kind)
 
     pieces = 4
@@ -300,29 +357,34 @@
     def part_of(h):
         return pl.ds(h * half, half)
 
-    def cross(h):
-        return copy(
-            v.over.at[part_of(h)], v.came.at[part_of(h)], v.cross_send, v.cross_recv.at[h],
-            peer_x,
-        )
-
-    for h in range(2):
-        at = slice(h * half, (h + 1) * half)
+    bands = v.cross_recv.shape[0]
+    band = kept // bands
+
+    def band_of(n):
+        return pl.ds(n * band, band)
+
+    def cross(n):
+        return copy(
+            v.over.at[band_of(n)], v.came.at[band_of(n)], v.cross_send, v.cross_recv.at[n], peer_x
+        )
+
+    for n in range(bands):
+        at = slice(n * band, (n + 1) * band)
         v.over[at, :] = (v.keep[0, at, :] + v.got[0, at, :].astype(single)).astype(kind)
-        cross(h).start()
+        cross(n).start()
 
     xs, part = (v.xs, v.part)
 
-    def ax(k, h):
-        return copy(
-            xs.at[k, 0, part_of(h)], xs.at[k, DX, part_of(h)], v.ax_send,
-            v.ax_recv.at[k, h], peer_x,
-        )
-
-    def ay(k, h):
-        return copy(
-            xs.at[k, 0, part_of(h)], xs.at[k, DY, part_of(h)], v.ay_send,
-            v.ay_recv.at[k, h], peer_y,
+    def ax(k, h, at=None):
+        at = part_of(h) if at is None else at
+        return copy(
+            xs.at[k, 0, at], xs.at[k, DX, at], v.ax_send, v.ax_recv.at[k, h], peer_x
+        )
+
+    def ay(k, h, at=None):
+        at = part_of(h) if at is None else at
+        return copy(
+            xs.at[k, 0, at], xs.at[k, DY, at], v.ay_send, v.ay_recv.at[k, h], peer_y
         )
 
     def fy(k):
@@ -358,9 +420,9 @@
     def landed(k):
         return all_of(xs.at[k, 0], v.az_recv.at[k])
 
-    for h in range(2):
-        at = slice(h * half, (h + 1) * half)
-        cross(h).wait_recv()
+    for n in range(bands):
+        at = slice(n * band, (n + 1) * band)
+        cross(n).wait_recv()
         total = v.keep[1, at, :] + v.got[1, at, :].astype(single) + v.came[at, :].astype(single)
         hidden = (v.stream[at, :].astype(single) + total).astype(kind)
         v.hidden[at, :] = hidden
@@ -368,18 +430,24 @@
         mean = jnp.mean(wide * wide, axis=-1, keepdims=True)
         normed = wide * lax.rsqrt(mean + NORM_EPSILON) * v.gain[...]
         xs[0, 0, at, :] = normed.astype(kind)
-        ax(0, h).start()
-        ay(0, h).start()
+        ax(0, n * 2 // bands, band_of(n)).start()
+        ay(0, n * 2 // bands, band_of(n)).start()
 
         @pl.when(z < depth - 1)
         def _():
-            upward(1, part_of(h)).start()
+            upward(1, band_of(n)).start()
 
         @pl.when(z > 0)
         def _():
-            downward(1, part_of(h)).start()
+            downward(1, band_of(n)).start()
 
     ac(0, 0).start()
+    all_of(v.weigh_in.at[others], v.weigh_recv).wait_recv()
+    table = v.weigh_out[sp]
+    for k in range(1, count):
+        table = table + v.weigh_in[k]
+    filled = jnp.concatenate([table, jnp.zeros((LANES - lines, rows), single)], axis=0)
+    v.weigh[...] = jnp.transpose(filled)
     for name in ("gate_w", "up_w", "down_w"):
         loads[name].wait()
 
@@ -513,50 +581,47 @@
         zr(k).start()
 
     def step(q, none):
-        k = nearest(z, q % depth, depth)
-        k_next = nearest(z, (q + 1) % depth, depth)
-        k_done = nearest(z, (q + depth - 1) % depth, depth)
-        k_older = nearest(z, (q + depth - 2) % depth, depth)
+        k = turn(z, q % depth, depth)
+        k_next = turn(z, (q + 1) % depth, depth)
+        k_done = turn(z, (q + depth - 1) % depth, depth)
+        k_older = turn(z, (q + depth - 2) % depth, depth)
         live, late = (q < depth, q > 0)
-
-        @pl.when(live)
-        def _():
-            spread_first(k)
 
         @pl.when(late)
         def _():
             all_of(xs.at[k_done, pl.ds(DC, DC)], v.ac_recv.at[k_done]).wait_recv()
             theirs(k_done)
 
+        @pl.when(live)
+        def _():
+            spread_first(k)
+
         @pl.when(q + 1 < depth)
         def _():
             relay(q + 1)
             enter(k_next)
 
+        @pl.when(q > 3)
+        def _():
+            reduce_next(k_older)
+
+        @pl.when(late)
+        def _():
+            ours(k_done)
+
+        @pl.when(q > 2)
+        def _():
+            reduce_first(k_done)
+
         @pl.when(live)
         def _():
             spread_rest(k)
-
-        @pl.when(q > 3)
-        def _():
-            reduce_next(k_older)
-
-        @pl.when(late)
-        def _():
-            ours(k_done)
-
-        @pl.when(q > 2)
-        def _():
-            reduce_first(k_done)
-
-        @pl.when(live)
-        def _():
             spread_last(k)
 
         return none
 
     lax.fori_loop(0, depth + 1, step, 0)
-    k_1, k_near, k_far = [nearest(z, p, depth) for p in (1, depth - 2, depth - 1)]
+    k_1, k_near, k_far = [turn(z, p, depth) for p in (1, depth - 2, depth - 1)]
     reduce_last(k_near)
     reduce_next(k_far)
     reduce_first(k_1)
@@ -633,7 +698,6 @@
     scratch.update(
         soft=pltpu.VMEM(decay.shape, single),
         gelu=flat,
-        head=pltpu.VMEM((SUBLANES, channels), single),
         halo=pltpu.VMEM((2 * SUBLANES, channels), kind),
         factor=flat,
         state=flat,
@@ -666,7 +730,7 @@
     sent = ("weigh", "end", "pair", "cross", "ax", "ay", "af", "ac", "rc", "rs", "rz")
     scratch.update({name + "_send": dma for name in sent})
     landing = dict(
-        weigh=(), end=(), pair=(), cross=(2,), ax=(depth, 2), ay=(depth, 2), af=(depth,),
+        weigh=(), end=(), pair=(), cross=(4,), ax=(depth, 2), ay=(depth, 2), af=(depth,),
         ac=(depth,), rc=(depth,), rs=(depth, 3), rz=(), az=(depth,),
     )
     scratch.update({name + "_recv": dma(shape) if shape else dma for name, shape in landing.items()})

time: 99.4 us -> 93.7 us (0.943)
  Pallas kernels: 97.6 us -> 91.9 us
    pallas_call x1, Pallas kernels: 97.6 us -> 91.9 us  [layer(): pl.pallas_call(functools.partial(layer_kernel, count, names), out_shape=j...]
where the time goes in v3:
time: 93.7 us; the launch traced here: 93.5 us
  Pallas kernels  91.9 us (98%)
  local copies, waits for them, and re-layouts  1.67 us (2%)
    pallas_call x1, Pallas kernels, layer(): pl.pallas_call(functools.partial(layer_kernel, count, names), out_shape=j...  91.9 us

profile of v3, /device:TPU:0, one launch (start us, length us, event | category | flops | bytes accessed | tf_op | source)
XLA Modules:
  0.0 93.5 jit_solution(6090687351713347881)
XLA Ops:
  0.0 91.9 %shard_map.145 = bf16[64,2048]{1,0:T(8,128)(2,1)} custom-call(bf16[256,512]{1,0:T(8,128)(2,1)} %refs_0_.1, bf16[256,512]{1,0:T(8,128)(2,1)} %refs_1_.1, f32[4,512]{1,0:T(4,128)} %refs_2_.1, bf16[2,2,128,128]{3,2,1,0:T(8,128)(2,1)} %refs_3_.1, bf16[2,1,256,256]{3,2,1,0:T(8,128)(2,1)} %refs_4_.1, f32[1,512]{1,0:T(1,128)} %bitcast.7, f32[256,512]{1,0:T(8,128)} %refs_6_.1, ...), custom_call_target="tpu_custom_call" | custom-call | tf_op jit(solution)/shard_map/pallas_call | solution.py:739
  91.9 1.7 %copy.17 = bf16[64,2048]{1,0:T(8,128)(2,1)} copy(bf16[64,2048]{1,0:T(8,128)(2,1)} %shard_map.145) | data formatting | bytes 524288

commit v4 on v3

--- a/solution.py
+++ b/solution.py
@@ -451,9 +451,11 @@
     for name in ("gate_w", "up_w", "down_w"):
         loads[name].wait()
 
-    def rc(k):
-        return copy(
-            part.at[k, pl.ds(DC, DC)], v.from_core.at[k], v.rc_send, v.rc_recv.at[k], peer_c
+    def rc(k, cols):
+        at = pl.ds(cols.start, cols.stop - cols.start)
+        return copy(
+            part.at[k, pl.ds(DC, DC), :, at], v.from_core.at[k, :, :, at], v.rc_send,
+            v.rc_recv.at[k], peer_c,
         )
 
     def rs(k, n):
@@ -470,9 +472,54 @@
             return copy(part.at[k, DX, part_of(0)], v.rest.at[k, 2], *sems, peer_x)
         return copy(part.at[k, DY, part_of(1)], v.rest.at[k, 3], *sems, peer_y)
 
-    def zr(k):
-        return copy(
-            part.at[k, 0], v.from_z.at[k], v.rz_send, v.rz_recv, plane(depth - k)
+    last = depth - 1
+    at_end = (z == 0) | (z == last)
+    beside = z + 1 - 2 * (z % 2)
+    inward = jnp.where(z == 0, 1, last - 1)
+    across = jnp.where(z == 1, last, 0)
+
+    bulk = v.from_pair.shape[1]
+    remnant = pl.ds(bulk, kept - bulk)
+    pair_device = {"sp": beside * 2 + y, "tp": tp}
+    over_y, over_x = (z * 2 + 1 - y, (1 - x) * 2 + c)
+    peer_1 = {"sp": (1 - c) * sp + c * over_y, "tp": (1 - c) * over_x + c * tp}
+    peer_2 = {"sp": (1 - c) * over_y + c * sp, "tp": (1 - c) * tp + c * over_x}
+
+    def to_pair(k):
+        return copy(
+            part.at[k, pl.ds(0, DC), pl.ds(0, bulk)], v.from_pair, v.rp_send, v.rp_recv,
+            pair_device,
+        )
+
+    def rq(k, n):
+        if n == 0:
+            there = part.at[k, DX + DY, remnant]
+            return copy(there, v.from_1, v.rq_send, v.rq_recv.at[0], peer_1)
+        if n == 1:
+            there = part.at[k, DX + c, remnant]
+            return copy(there, v.from_2.at[0], v.rq_send, v.rq_recv.at[1], peer_1)
+        if n == 2:
+            there = part.at[k, DY - c, remnant]
+            return copy(there, v.from_2.at[1], v.rq_send, v.rq_recv.at[1], peer_2)
+        return copy(part.at[k, 0, remnant], v.from_3, v.rq_send, v.rq_recv.at[2], pair_device)
+
+    def remnant_next(k):
+        rq(k, 0).wait_recv()
+        now = part[k, DY - c, bulk:kept].astype(single) + v.from_1[...].astype(single)
+        part[k, DY - c, bulk:kept] = now.astype(kind)
+        rq(k, 2).start()
+
+    def remnant_last(k):
+        all_of(v.from_2, v.rq_recv.at[1]).wait_recv()
+        now = part[k, 0, bulk:kept].astype(single) + v.from_2[0].astype(single)
+        part[k, 0, bulk:kept] = (now + v.from_2[1].astype(single)).astype(kind)
+        rq(k, 3).start()
+
+    def zr(p, k):
+        to = jnp.where(at_end, inward, across) if p == 2 else last - z
+        return copy(
+            part.at[k, 0], v.from_z.at[p - 2], v.rz_send, v.rz_recv.at[p - 2],
+            {"sp": to * 2 + y, "tp": tp},
         )
 
     lane = lax.broadcasted_iota(jnp.int32, (kept, LANES), 1)
@@ -497,17 +544,19 @@
         u = jnp.dot(rows_in, v.up_w[...], preferred_element_type=single)
         return (clamp_units(g, u) * share_of(k, j)).astype(kind)
 
-    def theirs(k):
-        act = activated(k, 1)
+    def theirs_first(k):
+        v.act[...] = activated(k, 1)
+
+    def theirs_next(k):
         for n in range(pieces):
             cols = slice(n * piece, (n + 1) * piece)
-            down = jnp.dot(act, v.down_w[:, cols], preferred_element_type=single)
+            down = jnp.dot(v.act[...], v.down_w[:, cols], preferred_element_type=single)
             part[k, DC : 2 * DC, :, cols] = down.astype(kind).reshape(DC, kept, piece)
-        rc(k).start()
+            rc(k, cols).start()
 
     def ours(k):
         act = activated(k, 0)
-        rc(k).wait_recv()
+        all_of(v.from_core.at[k], v.rc_recv.at[k]).wait_recv()
         for n in range(pieces):
             cols = slice(n * piece, (n + 1) * piece)
             down = jnp.dot(act, v.down_w[:, cols], preferred_element_type=single)
@@ -574,11 +623,19 @@
         lower = part[k, 0, half:kept].astype(single) + v.rest[k, 1].astype(single)
         return (upper + v.rest[k, 2].astype(single), lower + v.rest[k, 3].astype(single))
 
-    def reduce_last(k):
+    def reduce_last(p, k):
         upper, lower = reduced(k)
         part[k, 0, 0:half] = upper.astype(kind)
         part[k, 0, half:kept] = lower.astype(kind)
-        zr(k).start()
+        if p == 3:
+
+            @pl.when((z > 0) & (z < last))
+            def _():
+                all_of(v.from_z.at[0], v.rz_recv.at[0]).wait_recv()
+                now = part[k, 0].astype(single) + v.from_z[0].astype(single)
+                part[k, 0] = now.astype(kind)
+
+        zr(p, k).start()
 
     def step(q, none):
         k = turn(z, q % depth, depth)
@@ -590,11 +647,15 @@
         @pl.when(late)
         def _():
             all_of(xs.at[k_done, pl.ds(DC, DC)], v.ac_recv.at[k_done]).wait_recv()
-            theirs(k_done)
+            theirs_first(k_done)
 
         @pl.when(live)
         def _():
             spread_first(k)
+
+        @pl.when(late)
+        def _():
+            theirs_next(k_done)
 
         @pl.when(q + 1 < depth)
         def _():
@@ -609,6 +670,10 @@
         def _():
             ours(k_done)
 
+        @pl.when(q == 2)
+        def _():
+            to_pair(k_done).start()
+
         @pl.when(q > 2)
         def _():
             reduce_first(k_done)
@@ -621,41 +686,49 @@
         return none
 
     lax.fori_loop(0, depth + 1, step, 0)
-    k_1, k_near, k_far = [turn(z, p, depth) for p in (1, depth - 2, depth - 1)]
-    reduce_last(k_near)
+    k_pair, k_near, k_far = [turn(z, p, depth) for p in (1, 2, 3)]
+    reduce_last(2, k_near)
+    all_of(v.from_pair, v.rp_recv).wait_recv()
+    for n in range(DC):
+        now = part[0, n, 0:bulk].astype(single) + v.from_pair[n].astype(single)
+        part[0, n, 0:bulk] = now.astype(kind)
     reduce_next(k_far)
-    reduce_first(k_1)
-    reduce_last(k_far)
-    reduce_next(k_1)
+    rq(k_pair, 0).start()
+    rq(k_pair, 1).start()
     reduce_first(0)
-    reduce_last(k_1)
+    reduce_last(3, k_far)
+    remnant_next(k_pair)
     reduce_next(0)
+    remnant_last(k_pair)
     upper, lower = reduced(0)
     upper = upper + v.hidden[0:half, :].astype(single)
     lower = lower + v.hidden[half:kept, :].astype(single)
-    beyond = pl.ds(1, depth - 1)
-    all_of(v.from_z.at[beyond], v.rz_recv).wait_recv()
-    for k in range(1, depth):
-        upper = upper + v.from_z[k, 0:half].astype(single)
-        lower = lower + v.from_z[k, half:kept].astype(single)
-    results = []
+
+    @pl.when(at_end)
+    def _():
+        all_of(v.from_z.at[0], v.rz_recv.at[0]).wait_recv()
+
+    all_of(v.from_z.at[1], v.rz_recv.at[1]).wait_recv()
+    direct = jnp.where(at_end, 1.0, 0.0)
+    upper = upper + direct * v.from_z[0, 0:half].astype(single)
+    lower = lower + direct * v.from_z[0, half:kept].astype(single)
+    upper = upper + v.from_z[1, 0:half].astype(single)
+    lower = lower + v.from_z[1, half:kept].astype(single)
+    rq(k_pair, 3).wait_recv()
+    rest = jnp.concatenate(
+        [jnp.zeros((bulk - half, width), single), v.from_3[...].astype(single)], axis=0
+    )
+    lower = lower + rest
     for h, value in enumerate((upper, lower)):
-        v.result[h * half : (h + 1) * half, :] = value.astype(v.result.dtype)
-        results.append(
-            pltpu.make_async_copy(
-                v.result.at[part_of(h)], v.out.at[part_of(h)], v.result_sem.at[h]
-            )
-        )
-        results[h].start()
-
+        v.out[h * half : (h + 1) * half, :] = value.astype(v.out.dtype)
     every = pl.ds(0, depth)
     quarter = xs.at[every, pl.ds(0, 1)]
     for ref, sem in (
         (v.weigh_in.at[others], v.weigh_send), (v.ends.at[others], v.end_send),
         (v.give, v.pair_send), (v.over, v.cross_send), (quarter, v.ax_send),
         (quarter, v.ay_send), (quarter, v.af_send), (xs.at[every, pl.ds(0, DC)], v.ac_send),
-        (part.at[every, pl.ds(DC, DC)], v.rc_send), (part.at[every, pl.ds(0, 3)], v.rs_send),
-        (v.from_z.at[beyond], v.rz_send),
+        (part.at[every, pl.ds(DC, DC)], v.rc_send), (part.at[pl.ds(1, last), pl.ds(0, 3)], v.rs_send),
+        (v.from_z, v.rz_send), (v.from_pair, v.rp_send), (part.at[0, 0], v.rq_send),
     ):
         all_of(ref, sem).wait_send()
     for i in range(1, depth):
@@ -667,9 +740,6 @@
         @pl.when((z + i <= depth) & (z > 0))
         def _():
             downward(i, whole).wait_send()
-
-    for one in results:
-        one.wait()
 
 
 def layer(
@@ -682,6 +752,7 @@
     kept, width = stream.shape
     half = kept // 2
     pieces = 4
+    bulk = kept * 3 // 4
     lines = -(-count // SUBLANES) * SUBLANES
     single, kind = (jnp.float32, jnp.bfloat16)
     dma = pltpu.SemaphoreType.DMA
@@ -716,31 +787,34 @@
         came=pltpu.VMEM((kept, width), kind),
         hidden=pltpu.VMEM((kept, width), kind),
         xs=pltpu.VMEM((depth, 2 * DC, kept, width), kind),
+        act=pltpu.VMEM((DC * kept, expert_gate.shape[2]), kind),
         part=pltpu.VMEM((depth, 2 * DC, kept, width), kind),
         from_core=pltpu.VMEM((depth, DC, kept, width), kind),
         first=pltpu.VMEM((depth, 2, half, width), kind),
         rest=pltpu.VMEM((depth, 4, half, width), kind),
-        from_z=pltpu.VMEM((depth, kept, width), kind),
-        result=pltpu.VMEM((kept, width), kind),
+        from_z=pltpu.VMEM((2, kept, width), kind),
+        from_pair=pltpu.VMEM((DC, bulk, width), kind),
+        from_1=pltpu.VMEM((kept - bulk, width), kind),
+        from_2=pltpu.VMEM((2, kept - bulk, width), kind),
+        from_3=pltpu.VMEM((kept - bulk, width), kind),
         load_sem=dma((len(inputs),)),
-        result_sem=dma((2,)),
         halo_send=dma,
         halo_recv=dma,
     )
-    sent = ("weigh", "end", "pair", "cross", "ax", "ay", "af", "ac", "rc", "rs", "rz")
+    sent = ("weigh", "end", "pair", "cross", "ax", "ay", "af", "ac", "rc", "rs", "rz", "rp", "rq")
     scratch.update({name + "_send": dma for name in sent})
     landing = dict(
         weigh=(), end=(), pair=(), cross=(4,), ax=(depth, 2), ay=(depth, 2), af=(depth,),
-        ac=(depth,), rc=(depth,), rs=(depth, 3), rz=(), az=(depth,),
+        ac=(depth,), rc=(depth,), rs=(depth, 3), rz=(2,), rp=(), rq=(3,), az=(depth,),
     )
     scratch.update({name + "_recv": dma(shape) if shape else dma for name, shape in landing.items()})
     scratch.update(up_send=dma((depth,)), dn_send=dma((depth,)))
     names = [name + "_hbm" for name in inputs] + ["out"] + list(scratch)
     return pl.pallas_call(
         functools.partial(layer_kernel, count, names),
-        out_shape=jax.ShapeDtypeStruct((kept, width), kind),
+        out_shape=pltpu.VMEM((kept, width), kind),
         in_specs=[pl.BlockSpec(memory_space=pl.ANY)] * len(inputs),
-        out_specs=pl.BlockSpec(memory_space=pl.ANY),
+        out_specs=pl.BlockSpec(memory_space=pltpu.VMEM),
         scratch_shapes=list(scratch.values()),
         compiler_params=pltpu.CompilerParams(
             collective_id=1, has_side_effects=True, vmem_limit_bytes=60 * 1024 * 1024

time: 93.7 us -> 86.1 us (0.919)
  Pallas kernels: 91.9 us -> 84.7 us
  local copies, waits for them, and re-layouts: 1.67 us -> 0.71 us
    pallas_call x1, Pallas kernels: 91.9 us -> 84.7 us  [layer(): pl.pallas_call(functools.partial(layer_kernel, count, names), out_shape=p...]
    unnamed x1, local copies, waits for them, and re-layouts: 1.67 us -> 0.71 us
where the time goes in v4:
time: 86.1 us; the launch traced here: 85.4 us
  Pallas kernels  84.7 us (98%)
    pallas_call x1, Pallas kernels, layer(): pl.pallas_call(functools.partial(layer_kernel, count, names), out_shape=p...  84.7 us

profile of v4, /device:TPU:0, one launch (start us, length us, event | category | flops | bytes accessed | tf_op | source)
XLA Modules:
  0.0 85.4 jit_solution(8127576684162403552)
XLA Ops:
  0.0 84.7 %shard_map.145 = bf16[64,2048]{1,0:T(8,128)(2,1)S(1)} custom-call(bf16[256,512]{1,0:T(8,128)(2,1)} %refs_0_.1, bf16[256,512]{1,0:T(8,128)(2,1)} %refs_1_.1, f32[4,512]{1,0:T(4,128)} %refs_2_.1, bf16[2,2,128,128]{3,2,1,0:T(8,128)(2,1)} %refs_3_.1, bf16[2,1,256,256]{3,2,1,0:T(8,128)(2,1)} %refs_4_.1, f32[1,512]{1,0:T(1,128)} %bitcast.7, f32[256,512]{1,0:T(8,128)} %refs_6_.1, ...), custom_call_target="tpu_custom_call" | custom-call | tf_op jit(solution)/shard_map/pallas_call | solution.py:813
  84.7 0.7 copy.17

commit v5 on v4

--- a/solution.py
+++ b/solution.py
@@ -405,6 +405,21 @@
         )
 
     whole = pl.ds(0, kept)
+    beside = z + 1 - 2 * (z % 2)
+    pair_device = {"sp": beside * 2 + y, "tp": tp}
+    pair_slot = 1 + (z % 2) * (depth - 2)
+
+    def lift_x():
+        return copy(
+            xs.at[0, DX, part_of(0)], xs.at[pair_slot, DX, part_of(0)], v.ax_send,
+            v.ax_recv.at[pair_slot, 0], pair_device,
+        )
+
+    def lift_y():
+        return copy(
+            xs.at[0, DY, part_of(1)], xs.at[pair_slot, DY, part_of(1)], v.ay_send,
+            v.ay_recv.at[pair_slot, 1], pair_device,
+        )
 
     def upward(i, at):
         return copy(
@@ -474,13 +489,11 @@
 
     last = depth - 1
     at_end = (z == 0) | (z == last)
-    beside = z + 1 - 2 * (z % 2)
     inward = jnp.where(z == 0, 1, last - 1)
     across = jnp.where(z == 1, last, 0)
 
     bulk = v.from_pair.shape[1]
     remnant = pl.ds(bulk, kept - bulk)
-    pair_device = {"sp": beside * 2 + y, "tp": tp}
     over_y, over_x = (z * 2 + 1 - y, (1 - x) * 2 + c)
     peer_1 = {"sp": (1 - c) * sp + c * over_y, "tp": (1 - c) * over_x + c * tp}
     peer_2 = {"sp": (1 - c) * over_y + c * sp, "tp": (1 - c) * tp + c * over_x}
@@ -515,12 +528,72 @@
         part[k, 0, bulk:kept] = (now + v.from_2[1].astype(single)).astype(kind)
         rq(k, 3).start()
 
-    def zr(p, k):
-        to = jnp.where(at_end, inward, across) if p == 2 else last - z
-        return copy(
-            part.at[k, 0], v.from_z.at[p - 2], v.rz_send, v.rz_recv.at[p - 2],
-            {"sp": to * 2 + y, "tp": tp},
-        )
+    def zr_near(k):
+        to = jnp.where(at_end, inward, across)
+        return copy(
+            part.at[k, 0], v.from_z.at[0], v.rz_send, v.rz_recv.at[0], {"sp": to * 2 + y, "tp": tp}
+        )
+
+    small = half // 2
+
+    def slim(h, t):
+        return pl.ds(h * half + t * small, small)
+
+    def zr_far(k, h, t):
+        return copy(
+            part.at[k, 0, slim(h, t)], v.from_z.at[1, slim(h, t)], v.rz_send, v.rz_recv.at[1],
+            {"sp": (last - z) * 2 + y, "tp": tp},
+        )
+
+    def rt(k, t, n):
+        here = slim(0, t)
+        sems = (v.rs_send, v.rt_recv.at[t, min(n, 2)])
+        if n == 0:
+            return copy(part.at[k, DX + DY, here], v.first.at[k, 0, here], *sems, peer_y)
+        if n == 1:
+            return copy(part.at[k, DX + DY, slim(1, t)], v.first.at[k, 1, here], *sems, peer_x)
+        if n == 2:
+            return copy(part.at[k, DY, here], v.rest.at[k, 0, here], *sems, peer_y)
+        if n == 3:
+            return copy(part.at[k, DX, slim(1, t)], v.rest.at[k, 1, here], *sems, peer_x)
+        if n == 4:
+            return copy(part.at[k, DX, here], v.rest.at[k, 2, here], *sems, peer_x)
+        return copy(part.at[k, DY, slim(1, t)], v.rest.at[k, 3, here], *sems, peer_y)
+
+    def slim_next(k, t):
+        here = slice(t * small, (t + 1) * small)
+        there = slice(half + t * small, half + (t + 1) * small)
+        rt(k, t, 0).wait_recv()
+        now = part[k, DX, here].astype(single) + v.first[k, 0, here].astype(single)
+        part[k, DX, here] = now.astype(kind)
+        rt(k, t, 4).start()
+        rt(k, t, 1).wait_recv()
+        now = part[k, DY, there].astype(single) + v.first[k, 1, here].astype(single)
+        part[k, DY, there] = now.astype(kind)
+        rt(k, t, 5).start()
+
+    def slim_last(k, t):
+        here = slice(t * small, (t + 1) * small)
+        all_of(v.rest.at[k, pl.ds(0, 4), slim(0, t)], v.rt_recv.at[t, 2]).wait_recv()
+        inner = (z > 0) & (z < last)
+        if t == 0:
+
+            @pl.when(inner)
+            def _():
+                all_of(v.from_z.at[0], v.rz_recv.at[0]).wait_recv()
+
+        for h in range(2):
+            rows_h = slice(h * half + t * small, h * half + (t + 1) * small)
+            now = part[k, 0, rows_h].astype(single) + v.rest[k, h, here].astype(single)
+            now = now + v.rest[k, h + 2, here].astype(single)
+            part[k, 0, rows_h] = now.astype(kind)
+
+            @pl.when(inner)
+            def _():
+                more = part[k, 0, rows_h].astype(single) + v.from_z[0, rows_h].astype(single)
+                part[k, 0, rows_h] = more.astype(kind)
+
+            zr_far(k, h, t).start()
 
     lane = lax.broadcasted_iota(jnp.int32, (kept, LANES), 1)
 
@@ -563,7 +636,22 @@
             down = down.reshape(DC, kept, piece) + v.from_core[k, :, :, cols].astype(single)
             part[k, 0:DC, :, cols] = down.astype(kind)
 
-    def spread_first(k):
+    def spread_first(k, q):
+        ax(k, 0).wait_recv()
+        fy(k).start()
+
+        @pl.when((q == 0) & (c == 0))
+        def _():
+            lift_x().start()
+
+        ay(k, 1).wait_recv()
+        fx(k).start()
+
+        @pl.when((q == 0) & (c == 1))
+        def _():
+            lift_y().start()
+
+    def spread_second(k):
         ax(k, 0).wait_recv()
         fy(k).start()
         ay(k, 1).wait_recv()
@@ -596,9 +684,15 @@
             def _():
                 downward(i + 1, whole).start()
 
-    def enter(k):
-        ax(k, 0).start()
-        ay(k, 1).start()
+    def enter(k, q):
+        @pl.when((q > 0) | (c == 1))
+        def _():
+            ax(k, 0).start()
+
+        @pl.when((q > 0) | (c == 0))
+        def _():
+            ay(k, 1).start()
+
         ax(k, 1).start()
         ay(k, 0).start()
         ac(k, 0).start()
@@ -623,19 +717,11 @@
         lower = part[k, 0, half:kept].astype(single) + v.rest[k, 1].astype(single)
         return (upper + v.rest[k, 2].astype(single), lower + v.rest[k, 3].astype(single))
 
-    def reduce_last(p, k):
+    def reduce_last(k):
         upper, lower = reduced(k)
         part[k, 0, 0:half] = upper.astype(kind)
         part[k, 0, half:kept] = lower.astype(kind)
-        if p == 3:
-
-            @pl.when((z > 0) & (z < last))
-            def _():
-                all_of(v.from_z.at[0], v.rz_recv.at[0]).wait_recv()
-                now = part[k, 0].astype(single) + v.from_z[0].astype(single)
-                part[k, 0] = now.astype(kind)
-
-        zr(p, k).start()
+        zr_near(k).start()
 
     def step(q, none):
         k = turn(z, q % depth, depth)
@@ -644,59 +730,78 @@
         k_older = turn(z, (q + depth - 2) % depth, depth)
         live, late = (q < depth, q > 0)
 
+        @pl.when(q < last)
+        def _():
+            spread_first(k, q)
+
         @pl.when(late)
         def _():
             all_of(xs.at[k_done, pl.ds(DC, DC)], v.ac_recv.at[k_done]).wait_recv()
             theirs_first(k_done)
 
+        @pl.when(q == last)
+        def _():
+            spread_second(k)
+
+        @pl.when(late)
+        def _():
+            theirs_next(k_done)
+
+        @pl.when(q + 1 < depth)
+        def _():
+            relay(q + 1)
+            enter(k_next, q)
+            spread_rest(k)
+
+        @pl.when(q > 3)
+        def _():
+            reduce_next(k_older)
+
+        @pl.when(late)
+        def _():
+            ours(k_done)
+
+        @pl.when(q == 2)
+        def _():
+            to_pair(k_done).start()
+
+        @pl.when(q == last)
+        def _():
+            reduce_first(k_done)
+
+        @pl.when(q > last)
+        def _():
+            for n in range(4):
+                rt(k_done, 0, n).start()
+            rt(k_done, 1, 0).start()
+            rt(k_done, 1, 1).start()
+
+        @pl.when(q == last)
+        def _():
+            spread_rest(k)
+
         @pl.when(live)
         def _():
-            spread_first(k)
-
-        @pl.when(late)
-        def _():
-            theirs_next(k_done)
-
-        @pl.when(q + 1 < depth)
-        def _():
-            relay(q + 1)
-            enter(k_next)
-
-        @pl.when(q > 3)
-        def _():
-            reduce_next(k_older)
-
-        @pl.when(late)
-        def _():
-            ours(k_done)
-
-        @pl.when(q == 2)
-        def _():
-            to_pair(k_done).start()
-
-        @pl.when(q > 2)
-        def _():
-            reduce_first(k_done)
-
-        @pl.when(live)
-        def _():
-            spread_rest(k)
             spread_last(k)
 
         return none
 
     lax.fori_loop(0, depth + 1, step, 0)
     k_pair, k_near, k_far = [turn(z, p, depth) for p in (1, 2, 3)]
-    reduce_last(2, k_near)
+    reduce_last(k_near)
+    slim_next(k_far, 0)
+    rt(k_far, 1, 2).start()
+    rt(k_far, 1, 3).start()
     all_of(v.from_pair, v.rp_recv).wait_recv()
     for n in range(DC):
         now = part[0, n, 0:bulk].astype(single) + v.from_pair[n].astype(single)
         part[0, n, 0:bulk] = now.astype(kind)
-    reduce_next(k_far)
+    slim_next(k_far, 1)
     rq(k_pair, 0).start()
     rq(k_pair, 1).start()
     reduce_first(0)
-    reduce_last(3, k_far)
+    slim_last(k_far, 0)
+    slim_last(k_far, 1)
     remnant_next(k_pair)
     reduce_next(0)
     remnant_last(k_pair)
@@ -805,7 +910,7 @@
     scratch.update({name + "_send": dma for name in sent})
     landing = dict(
         weigh=(), end=(), pair=(), cross=(4,), ax=(depth, 2), ay=(depth, 2), af=(depth,),
-        ac=(depth,), rc=(depth,), rs=(depth, 3), rz=(2,), rp=(), rq=(3,), az=(depth,),
+        ac=(depth,), rc=(depth,), rs=(depth, 3), rz=(2,), rp=(), rq=(3,), az=(depth,), rt=(2, 3),
     )
     scratch.update({name + "_recv": dma(shape) if shape else dma for name, shape in landing.items()})
     scratch.update(up_send=dma((depth,)), dn_send=dma((depth,)))

time: 86.1 us -> 84.3 us (0.979)
  Pallas kernels: 84.7 us -> 83.5 us
    pallas_call x1, Pallas kernels: 84.7 us -> 83.5 us  [layer(): pl.pallas_call(functools.partial(layer_kernel, count, names), out_shape=p...]
where the time goes in v5:
time: 84.3 us; the launch traced here: 84.2 us
  Pallas kernels  83.5 us (99%)
    pallas_call x1, Pallas kernels, layer(): pl.pallas_call(functools.partial(layer_kernel, count, names), out_shape=p...  83.5 us

profile of v5, /device:TPU:0, one launch (start us, length us, event | category | flops | bytes accessed | tf_op | source)
XLA Modules:
  0.0 84.2 jit_solution(5834220796153113970)
XLA Ops:
  0.0 83.5 %shard_map.145 = bf16[64,2048]{1,0:T(8,128)(2,1)S(1)} custom-call(bf16[256,512]{1,0:T(8,128)(2,1)} %refs_0_.1, bf16[256,512]{1,0:T(8,128)(2,1)} %refs_1_.1, f32[4,512]{1,0:T(4,128)} %refs_2_.1, bf16[2,2,128,128]{3,2,1,0:T(8,128)(2,1)} %refs_3_.1, bf16[2,1,256,256]{3,2,1,0:T(8,128)(2,1)} %refs_4_.1, f32[1,512]{1,0:T(1,128)} %bitcast.7, f32[256,512]{1,0:T(8,128)} %refs_6_.1, ...), custom_call_target="tpu_custom_call" | custom-call | tf_op jit(solution)/shard_map/pallas_call | solution.py:918
  83.5 0.7 copy.17

commit v6 on v5

--- a/solution.py
+++ b/solution.py
@@ -183,7 +183,7 @@
         return copy(ref, ref, sem, sem, peer_c)
 
     barrier = pltpu.get_barrier_semaphore()
-    peers = [peer_x, peer_c] + [later(k) for k in range(1, count)]
+    peers = [later(k) for k in range(count - 1, 0, -1)] + [peer_x, peer_c]
     for peer in peers:
         pl.semaphore_signal(barrier, inc=1, device_id=peer, device_id_type=mesh_id)
     load_names = (
@@ -288,7 +288,7 @@
         v.ends[0, groups + n : groups + n + 1, :] = end_state[:, cols]
     end_copies = [
         copy(v.ends.at[0], v.ends.at[k], v.end_send, v.end_recv, later(k))
-        for k in range(1, count)
+        for k in range(count - 1, 0, -1)
     ]
     for one in end_copies:
         one.start()
@@ -328,35 +328,29 @@
         carry = jnp.where(sp >= k, longer, carry)
     carry = jnp.concatenate([carry[n : n + 1, :] for n in range(groups)], axis=1)
     beyond_lead = lead_state + lead_factor * carry
-    row = lax.broadcasted_iota(jnp.int32, (kept, channels), 0)
+    row = lax.broadcasted_iota(jnp.int32, (half, channels), 0)
     order = [(1 - x, 1 - c), (x, 1 - c), (1 - x, c), (x, c)]
-    for n, (chip, core) in enumerate(order):
-        first = (chip * 2 + core) * kept
-        at = pl.ds(pl.multiple_of(first, kept), kept)
-        entering = jnp.where(row + first < lead, carry, beyond_lead)
-        recurrent = v.state[at, :] + v.factor[at, :] * entering
-        v.gated[n * kept : (n + 1) * kept, :] = (recurrent * v.gelu[at, :]).astype(kind)
+    for h in range(2):
+        for n, (chip, core) in enumerate(order):
+            first = (chip * 2 + core) * kept + h * half
+            at = pl.ds(pl.multiple_of(first, half), half)
+            entering = jnp.where(row + first < lead, carry, beyond_lead)
+            recurrent = v.state[at, :] + v.factor[at, :] * entering
+            to = (4 * h + n) * half
+            v.gated[to : to + half, :] = (recurrent * v.gelu[at, :]).astype(kind)
 
     pieces = 4
     piece = width // pieces
 
-    def pair(n):
-        cols = pl.ds(n * piece, piece)
-        return copy(
-            v.give.at[:, :, cols], v.got.at[:, :, cols], v.pair_send, v.pair_recv, peer_c
-        )
-
-    for n in range(pieces):
-        cols = slice(n * piece, (n + 1) * piece)
-        value = jnp.dot(v.gated[...], v.mixer[:, cols], preferred_element_type=single)
-        v.give[:, :, cols] = value[: 2 * kept].astype(kind).reshape(2, kept, piece)
-        v.keep[:, :, cols] = value[2 * kept :].reshape(2, kept, piece)
-        pair(n).start()
-    all_of(v.got, v.pair_recv).wait_recv()
-
     def part_of(h):
         return pl.ds(h * half, half)
 
+    def pair(h):
+        return copy(
+            v.give.at[:, part_of(h)], v.got.at[:, part_of(h)], v.pair_send, v.pair_recv.at[h],
+            peer_c,
+        )
+
     bands = v.cross_recv.shape[0]
     band = kept // bands
 
@@ -368,24 +362,47 @@
             v.over.at[band_of(n)], v.came.at[band_of(n)], v.cross_send, v.cross_recv.at[n], peer_x
         )
 
-    for n in range(bands):
-        at = slice(n * band, (n + 1) * band)
-        v.over[at, :] = (v.keep[0, at, :] + v.got[0, at, :].astype(single)).astype(kind)
-        cross(n).start()
+    def send_across(h):
+        pair(h).wait_recv()
+        for n in range(h * bands // 2, (h + 1) * bands // 2):
+            at = slice(n * band, (n + 1) * band)
+            v.over[at, :] = (v.keep[0, at, :] + v.got[0, at, :].astype(single)).astype(kind)
+            cross(n).start()
+
+    for h in range(2):
+        at = slice(h * half, (h + 1) * half)
+        for n in range(pieces):
+            cols = slice(n * piece, (n + 1) * piece)
+            value = jnp.dot(
+                v.gated[4 * h * half : 4 * (h + 1) * half, :], v.mixer[:, cols],
+                preferred_element_type=single,
+            )
+            v.give[:, at, cols] = value[: 2 * half].astype(kind).reshape(2, half, piece)
+            v.keep[:, at, cols] = value[2 * half :].reshape(2, half, piece)
+        pair(h).start()
+        if h == 0:
+
+            @pl.when(c == 0)
+            def _():
+                send_across(0)
+
+    @pl.when(c == 1)
+    def _():
+        send_across(0)
+
+    send_across(1)
 
     xs, part = (v.xs, v.part)
 
-    def ax(k, h, at=None):
+    def ax(k, h, at=None, sem=None):
         at = part_of(h) if at is None else at
-        return copy(
-            xs.at[k, 0, at], xs.at[k, DX, at], v.ax_send, v.ax_recv.at[k, h], peer_x
-        )
-
-    def ay(k, h, at=None):
+        sem = v.ax_send if sem is None else sem
+        return copy(xs.at[k, 0, at], xs.at[k, DX, at], sem, v.ax_recv.at[k, h], peer_x)
+
+    def ay(k, h, at=None, sem=None):
         at = part_of(h) if at is None else at
-        return copy(
-            xs.at[k, 0, at], xs.at[k, DY, at], v.ay_send, v.ay_recv.at[k, h], peer_y
-        )
+        sem = v.ay_send if sem is None else sem
+        return copy(xs.at[k, 0, at], xs.at[k, DY, at], sem, v.ay_recv.at[k, h], peer_y)
 
     def fy(k):
         return copy(
@@ -528,20 +545,24 @@
         part[k, 0, bulk:kept] = (now + v.from_2[1].astype(single)).astype(kind)
         rq(k, 3).start()
 
-    def zr_near(k):
-        to = jnp.where(at_end, inward, across)
-        return copy(
-            part.at[k, 0], v.from_z.at[0], v.rz_send, v.rz_recv.at[0], {"sp": to * 2 + y, "tp": tp}
-        )
-
     small = half // 2
 
     def slim(h, t):
         return pl.ds(h * half + t * small, small)
 
+    def zr_near(k, h, t):
+        to = jnp.where(at_end, inward, across)
+        return copy(
+            part.at[k, 0, slim(h, t)], v.from_z.at[0, slim(h, t)], v.rz_send, v.rz_recv.at[t],
+            {"sp": to * 2 + y, "tp": tp},
+        )
+
+    def near_landed(t):
+        all_of(v.from_z.at[0, pl.ds(0, half)], v.rz_recv.at[t]).wait_recv()
+
     def zr_far(k, h, t):
         return copy(
-            part.at[k, 0, slim(h, t)], v.from_z.at[1, slim(h, t)], v.rz_send, v.rz_recv.at[1],
+            part.at[k, 0, slim(h, t)], v.from_z.at[1, slim(h, t)], v.rz_send, v.rz_recv.at[2],
             {"sp": (last - z) * 2 + y, "tp": tp},
         )
 
@@ -576,11 +597,10 @@
         here = slice(t * small, (t + 1) * small)
         all_of(v.rest.at[k, pl.ds(0, 4), slim(0, t)], v.rt_recv.at[t, 2]).wait_recv()
         inner = (z > 0) & (z < last)
-        if t == 0:
-
-            @pl.when(inner)
-            def _():
-                all_of(v.from_z.at[0], v.rz_recv.at[0]).wait_recv()
+
+        @pl.when(inner)
+        def _():
+            near_landed(t)
 
         for h in range(2):
             rows_h = slice(h * half + t * small, h * half + (t + 1) * small)
@@ -636,6 +656,32 @@
             down = down.reshape(DC, kept, piece) + v.from_core[k, :, :, cols].astype(single)
             part[k, 0:DC, :, cols] = down.astype(kind)
 
+    far_slot = 1 + (1 - z % 2) * (depth - 2)
+    inner_device = {"sp": (depth - 1 - z) * 2 + y, "tp": tp}
+
+    def haul_x(k, n):
+        return copy(
+            xs.at[k, DX, part_of(0)], xs.at[far_slot, DX, part_of(0)], v.haul_send.at[n],
+            v.ax_recv.at[far_slot, 0], inner_device if n == 0 else pair_device,
+        )
+
+    def haul_y(k, n):
+        return copy(
+            xs.at[k, DY, part_of(1)], xs.at[far_slot, DY, part_of(1)], v.haul_send.at[n],
+            v.ay_recv.at[far_slot, 1], inner_device if n == 0 else pair_device,
+        )
+
+    def haul(k, n):
+        inner = (z > 0) & (z < depth - 1)
+
+        @pl.when(inner & (c == 0))
+        def _():
+            haul_x(k, n).start()
+
+        @pl.when(inner & (c == 1))
+        def _():
+            haul_y(k, n).start()
+
     def spread_first(k, q):
         ax(k, 0).wait_recv()
         fy(k).start()
@@ -685,16 +731,32 @@
                 downward(i + 1, whole).start()
 
     def enter(k, q):
-        @pl.when((q > 0) | (c == 1))
+        @pl.when((q == 1) | ((q == 0) & (c == 1)))
         def _():
             ax(k, 0).start()
 
-        @pl.when((q > 0) | (c == 0))
+        @pl.when((q == 1) | ((q == 0) & (c == 0)))
         def _():
             ay(k, 1).start()
 
-        ax(k, 1).start()
-        ay(k, 0).start()
+        @pl.when((q == 2) & (c == 1))
+        def _():
+            ax(k, 0, sem=v.odd_send).start()
+
+        @pl.when((q == 2) & (c == 0))
+        def _():
+            ay(k, 1, sem=v.odd_send).start()
+
+        @pl.when(q < 2)
+        def _():
+            ax(k, 1).start()
+            ay(k, 0).start()
+
+        @pl.when(q == 2)
+        def _():
+            ax(k, 1, sem=v.odd_send).start()
+            ay(k, 0, sem=v.odd_send).start()
+
         ac(k, 0).start()
 
     def reduce_first(k):
@@ -721,7 +783,9 @@
         upper, lower = reduced(k)
         part[k, 0, 0:half] = upper.astype(kind)
         part[k, 0, half:kept] = lower.astype(kind)
-        zr_near(k).start()
+        for t in range(2):
+            for h in range(2):
+                zr_near(k, h, t).start()
 
     def step(q, none):
         k = turn(z, q % depth, depth)
@@ -734,6 +798,14 @@
         def _():
             spread_first(k, q)
 
+        @pl.when(q == 1)
+        def _():
+            haul(0, 0)
+
+        @pl.when(q == 2)
+        def _():
+            haul(k, 1)
+
         @pl.when(late)
         def _():
             all_of(xs.at[k_done, pl.ds(DC, DC)], v.ac_recv.at[k_done]).wait_recv()
@@ -742,6 +814,8 @@
         @pl.when(q == last)
         def _():
             spread_second(k)
+            rq(turn(z, 1, depth), 0).start()
+            rq(turn(z, 1, depth), 1).start()
 
         @pl.when(late)
         def _():
@@ -797,23 +871,22 @@
         now = part[0, n, 0:bulk].astype(single) + v.from_pair[n].astype(single)
         part[0, n, 0:bulk] = now.astype(kind)
     slim_next(k_far, 1)
-    rq(k_pair, 0).start()
-    rq(k_pair, 1).start()
+    remnant_next(k_pair)
     reduce_first(0)
     slim_last(k_far, 0)
     slim_last(k_far, 1)
-    remnant_next(k_pair)
+    remnant_last(k_pair)
     reduce_next(0)
-    remnant_last(k_pair)
     upper, lower = reduced(0)
     upper = upper + v.hidden[0:half, :].astype(single)
     lower = lower + v.hidden[half:kept, :].astype(single)
 
     @pl.when(at_end)
     def _():
-        all_of(v.from_z.at[0], v.rz_recv.at[0]).wait_recv()
-
-    all_of(v.from_z.at[1], v.rz_recv.at[1]).wait_recv()
+        for t in range(2):
+            near_landed(t)
+
+    all_of(v.from_z.at[1], v.rz_recv.at[2]).wait_recv()
     direct = jnp.where(at_end, 1.0, 0.0)
     upper = upper + direct * v.from_z[0, 0:half].astype(single)
     lower = lower + direct * v.from_z[0, half:kept].astype(single)
@@ -827,15 +900,21 @@
     for h, value in enumerate((upper, lower)):
         v.out[h * half : (h + 1) * half, :] = value.astype(v.out.dtype)
     every = pl.ds(0, depth)
-    quarter = xs.at[every, pl.ds(0, 1)]
+    quarter, six = (xs.at[every, pl.ds(0, 1)], v.first.at[pl.ds(0, 3)])
     for ref, sem in (
         (v.weigh_in.at[others], v.weigh_send), (v.ends.at[others], v.end_send),
-        (v.give, v.pair_send), (v.over, v.cross_send), (quarter, v.ax_send),
-        (quarter, v.ay_send), (quarter, v.af_send), (xs.at[every, pl.ds(0, DC)], v.ac_send),
+        (v.give, v.pair_send), (v.over, v.cross_send), (six, v.ax_send),
+        (six, v.ay_send), (v.rest.at[0, pl.ds(0, 3)], v.odd_send), (quarter, v.af_send), (xs.at[every, pl.ds(0, DC)], v.ac_send),
         (part.at[every, pl.ds(DC, DC)], v.rc_send), (part.at[pl.ds(1, last), pl.ds(0, 3)], v.rs_send),
         (v.from_z, v.rz_send), (v.from_pair, v.rp_send), (part.at[0, 0], v.rq_send),
     ):
         all_of(ref, sem).wait_send()
+
+    @pl.when((z > 0) & (z < last))
+    def _():
+        for n in range(2):
+            haul_x(0, n).wait_send()
+
     for i in range(1, depth):
 
         @pl.when((i - 1 <= z) & (z < depth - 1))
@@ -909,11 +988,13 @@
     sent = ("weigh", "end", "pair", "cross", "ax", "ay", "af", "ac", "rc", "rs", "rz", "rp", "rq")
     scratch.update({name + "_send": dma for name in sent})
     landing = dict(
-        weigh=(), end=(), pair=(), cross=(4,), ax=(depth, 2), ay=(depth, 2), af=(depth,),
-        ac=(depth,), rc=(depth,), rs=(depth, 3), rz=(2,), rp=(), rq=(3,), az=(depth,), rt=(2, 3),
+        weigh=(), end=(), pair=(2,), cross=(4,), ax=(depth, 2), ay=(depth, 2), af=(depth,),
+        ac=(depth,), rc=(depth,), rs=(depth, 3), rz=(3,), rp=(), rq=(3,), az=(depth,), rt=(2, 3),
     )
     scratch.update({name + "_recv": dma(shape) if shape else dma for name, shape in landing.items()})
-    scratch.update(up_send=dma((depth,)), dn_send=dma((depth,)))
+    scratch.update(
+        up_send=dma((depth,)), dn_send=dma((depth,)), haul_send=dma((2,)), odd_send=dma
+    )
     names = [name + "_hbm" for name in inputs] + ["out"] + list(scratch)
     return pl.pallas_call(
         functools.partial(layer_kernel, count, names),

time: 84.3 us -> 82.7 us (0.981)
  Pallas kernels: 83.5 us -> 81.8 us
    pallas_call x1, Pallas kernels: 83.5 us -> 81.8 us  [layer(): pl.pallas_call(functools.partial(layer_kernel, count, names), out_shape=p...]
where the time goes in v6:
time: 82.7 us; the launch traced here: 82.5 us
  Pallas kernels  81.8 us (99%)
    pallas_call x1, Pallas kernels, layer(): pl.pallas_call(functools.partial(layer_kernel, count, names), out_shape=p...  81.8 us

profile of v6, /device:TPU:0, one launch (start us, length us, event | category | flops | bytes accessed | tf_op | source)
XLA Modules:
  0.0 82.5 jit_solution(14110895929319644325)
XLA Ops:
  0.0 81.8 %shard_map.145 = bf16[64,2048]{1,0:T(8,128)(2,1)S(1)} custom-call(bf16[256,512]{1,0:T(8,128)(2,1)} %refs_0_.1, bf16[256,512]{1,0:T(8,128)(2,1)} %refs_1_.1, f32[4,512]{1,0:T(4,128)} %refs_2_.1, bf16[2,2,128,128]{3,2,1,0:T(8,128)(2,1)} %refs_3_.1, bf16[2,1,256,256]{3,2,1,0:T(8,128)(2,1)} %refs_4_.1, f32[1,512]{1,0:T(1,128)} %bitcast.7, f32[256,512]{1,0:T(8,128)} %refs_6_.1, ...), custom_call_target="tpu_custom_call" | custom-call | tf_op jit(solution)/shard_map/pallas_call | solution.py:999
  81.8 0.7 copy.17

commit v7 on v6

--- a/solution.py
+++ b/solution.py
@@ -647,12 +647,15 @@
             part[k, DC : 2 * DC, :, cols] = down.astype(kind).reshape(DC, kept, piece)
             rc(k, cols).start()
 
-    def ours(k):
-        act = activated(k, 0)
+    def ours(k, q):
+        @pl.when(q != last)
+        def _():
+            v.own_act[...] = activated(k, 0)
+
         all_of(v.from_core.at[k], v.rc_recv.at[k]).wait_recv()
         for n in range(pieces):
             cols = slice(n * piece, (n + 1) * piece)
-            down = jnp.dot(act, v.down_w[:, cols], preferred_element_type=single)
+            down = jnp.dot(v.own_act[...], v.down_w[:, cols], preferred_element_type=single)
             down = down.reshape(DC, kept, piece) + v.from_core[k, :, :, cols].astype(single)
             part[k, 0:DC, :, cols] = down.astype(kind)
 
@@ -660,15 +663,17 @@
     inner_device = {"sp": (depth - 1 - z) * 2 + y, "tp": tp}
 
     def haul_x(k, n):
-        return copy(
-            xs.at[k, DX, part_of(0)], xs.at[far_slot, DX, part_of(0)], v.haul_send.at[n],
-            v.ax_recv.at[far_slot, 0], inner_device if n == 0 else pair_device,
+        at = part_of(n // 2)
+        return copy(
+            xs.at[k, DX, at], xs.at[far_slot, DX, at], v.haul_send.at[n],
+            v.ax_recv.at[far_slot, n // 2], pair_device if n % 2 else inner_device,
         )
 
     def haul_y(k, n):
-        return copy(
-            xs.at[k, DY, part_of(1)], xs.at[far_slot, DY, part_of(1)], v.haul_send.at[n],
-            v.ay_recv.at[far_slot, 1], inner_device if n == 0 else pair_device,
+        at = part_of(1 - n // 2)
+        return copy(
+            xs.at[k, DY, at], xs.at[far_slot, DY, at], v.haul_send.at[n],
+            v.ay_recv.at[far_slot, 1 - n // 2], pair_device if n % 2 else inner_device,
         )
 
     def haul(k, n):
@@ -742,20 +747,17 @@
         @pl.when((q == 2) & (c == 1))
         def _():
             ax(k, 0, sem=v.odd_send).start()
+            ax(k, 1, sem=v.odd_send).start()
 
         @pl.when((q == 2) & (c == 0))
         def _():
             ay(k, 1, sem=v.odd_send).start()
+            ay(k, 0, sem=v.odd_send).start()
 
         @pl.when(q < 2)
         def _():
             ax(k, 1).start()
             ay(k, 0).start()
-
-        @pl.when(q == 2)
-        def _():
-            ax(k, 1, sem=v.odd_send).start()
-            ay(k, 0, sem=v.odd_send).start()
 
         ac(k, 0).start()
 
@@ -801,10 +803,17 @@
         @pl.when(q == 1)
         def _():
             haul(0, 0)
+            haul(0, 2)
 
         @pl.when(q == 2)
         def _():
             haul(k, 1)
+
+        @pl.when(q == last)
+        def _():
+            rq(turn(z, 1, depth), 0).start()
+            rq(turn(z, 1, depth), 1).start()
+            v.own_act[...] = activated(k_done, 0)
 
         @pl.when(late)
         def _():
@@ -814,8 +823,6 @@
         @pl.when(q == last)
         def _():
             spread_second(k)
-            rq(turn(z, 1, depth), 0).start()
-            rq(turn(z, 1, depth), 1).start()
 
         @pl.when(late)
         def _():
@@ -827,13 +834,17 @@
             enter(k_next, q)
             spread_rest(k)
 
+        @pl.when(q == 2)
+        def _():
+            haul(k, 3)
+
         @pl.when(q > 3)
         def _():
             reduce_next(k_older)
 
         @pl.when(late)
         def _():
-            ours(k_done)
+            ours(k_done, q)
 
         @pl.when(q == 2)
         def _():
@@ -904,7 +915,7 @@
     for ref, sem in (
         (v.weigh_in.at[others], v.weigh_send), (v.ends.at[others], v.end_send),
         (v.give, v.pair_send), (v.over, v.cross_send), (six, v.ax_send),
-        (six, v.ay_send), (v.rest.at[0, pl.ds(0, 3)], v.odd_send), (quarter, v.af_send), (xs.at[every, pl.ds(0, DC)], v.ac_send),
+        (six, v.ay_send), (v.rest.at[0, pl.ds(0, 2)], v.odd_send), (quarter, v.af_send), (xs.at[every, pl.ds(0, DC)], v.ac_send),
         (part.at[every, pl.ds(DC, DC)], v.rc_send), (part.at[pl.ds(1, last), pl.ds(0, 3)], v.rs_send),
         (v.from_z, v.rz_send), (v.from_pair, v.rp_send), (part.at[0, 0], v.rq_send),
     ):
@@ -912,7 +923,7 @@
 
     @pl.when((z > 0) & (z < last))
     def _():
-        for n in range(2):
+        for n in range(4):
             haul_x(0, n).wait_send()
 
     for i in range(1, depth):
@@ -972,6 +983,7 @@
         hidden=pltpu.VMEM((kept, width), kind),
         xs=pltpu.VMEM((depth, 2 * DC, kept, width), kind),
         act=pltpu.VMEM((DC * kept, expert_gate.shape[2]), kind),
+        own_act=pltpu.VMEM((DC * kept, expert_gate.shape[2]), kind),
         part=pltpu.VMEM((depth, 2 * DC, kept, width), kind),
         from_core=pltpu.VMEM((depth, DC, kept, width), kind),
         first=pltpu.VMEM((depth, 2, half, width), kind),
@@ -993,7 +1005,7 @@
     )
     scratch.update({name + "_recv": dma(shape) if shape else dma for name, shape in landing.items()})
     scratch.update(
-        up_send=dma((depth,)), dn_send=dma((depth,)), haul_send=dma((2,)), odd_send=dma
+        up_send=dma((depth,)), dn_send=dma((depth,)), haul_send=dma((4,)), odd_send=dma
     )
     names = [name + "_hbm" for name in inputs] + ["out"] + list(scratch)
     return pl.pallas_call(

time: 82.7 us -> 82.4 us (level)
  no operation moved by 1% of the time
where the time goes in v7:
time: 82.4 us; the launch traced here: 82.3 us
  Pallas kernels  81.6 us (99%)
    pallas_call x1, Pallas kernels, layer(): pl.pallas_call(functools.partial(layer_kernel, count, names), out_shape=p...  81.6 us

profile of v7, /device:TPU:0, one launch (start us, length us, event | category | flops | bytes accessed | tf_op | source)
XLA Modules:
  0.0 82.3 jit_solution(11761798907322797666)
XLA Ops:
  0.0 81.6 %shard_map.145 = bf16[64,2048]{1,0:T(8,128)(2,1)S(1)} custom-call(bf16[256,512]{1,0:T(8,128)(2,1)} %refs_0_.1, bf16[256,512]{1,0:T(8,128)(2,1)} %refs_1_.1, f32[4,512]{1,0:T(4,128)} %refs_2_.1, bf16[2,2,128,128]{3,2,1,0:T(8,128)(2,1)} %refs_3_.1, bf16[2,1,256,256]{3,2,1,0:T(8,128)(2,1)} %refs_4_.1, f32[1,512]{1,0:T(1,128)} %bitcast.7, f32[256,512]{1,0:T(8,128)} %refs_6_.1, ...), custom_call_target="tpu_custom_call" | custom-call | tf_op jit(solution)/shard_map/pallas_call | solution.py:1011
  81.6 0.7 copy.17
